TPU v7x, 32 devices: a whole 2x2x4 slice. The times are simulated.
32 devices in a mesh: sp: 8 (over z, x), tp: 4 (over y, core).
Axes of the slice: x: 2, y: 2, z: 4, core: 2. Of those that a mesh axis runs over, the one named last changes fastest.
Arguments:
- queries: bfloat16 [1536, 1536], P('sp', 'tp'), may hold values from -64 to 64
- latents: bfloat16 [1536, 512], P('sp'), may hold values from -6 to 6
- rope_key: bfloat16 [1536, 32], P('sp'), may hold values from -64 to 64
- w_key: bfloat16 [512, 1024], P(None, 'tp'), may hold values from -0.25 to 0.25
- w_value: bfloat16 [512, 1024], P(None, 'tp'), may hold values from -0.25 to 0.25
- w_out: bfloat16 [1024, 2048], P('tp'), may hold values from -0.59765625 to 0.59765625
- resid: bfloat16 [1536, 2048], P('sp', 'tp'), may hold values from -12 to 12
- gain_mix: float32 [2048], P('tp'), may hold values from 0.1 to 1.9
- w_gate: bfloat16 [2048, 3072], P('sp', 'tp'), may hold values from -0.125 to 0.125
- w_up: bfloat16 [2048, 3072], P('sp', 'tp'), may hold values from -0.125 to 0.125
- w_down: bfloat16 [3072, 2048], P('tp', 'sp'), may hold values from -0.41992188 to 0.41992188
- gain_out: float32 [2048], P('tp'), may hold values from 0.1 to 1.9
Outputs:
- layer_out: bfloat16 [1536, 2048], P('sp', 'tp')
All inputs are finite; a program needn't handle non-finite values.
Results may differ from a plain program's by a relative error of at most 0.014.
Values may be sent and summed in bfloat16 or wider, within the bound.
A program may use at most 128 MiB of HBM per device.

v0:
```python
import functools

import jax
import jax.numpy as jnp
from jax import lax
from jax.experimental import pallas as pl
from jax.experimental.pallas import tpu as pltpu
from jax.sharding import PartitionSpec as P

NOPE = 64
ROPE = 32
VDIM = 64
GRID_W = 64
LANES = 128

ROTARY_BASE = 10000.0
NORM_EPSILON = 1e-06
DEEP_ALPHA = 8.0**0.25
HALF_STEP = 0.5
MESH = pl.DeviceIdType.MESH


def rotary_tables(first, rows):
    at = first + lax.broadcasted_iota(jnp.int32, (rows, LANES), 0)
    column = lax.broadcasted_iota(jnp.int32, (rows, LANES), 1)
    freq_count = ROPE // 4
    grid_row = (at // GRID_W).astype(jnp.float32)
    grid_col = (at % GRID_W).astype(jnp.float32)
    spot = jnp.where(column % (2 * freq_count) < freq_count, grid_row, grid_col)
    inverse = jnp.ones((rows, LANES), jnp.float32)
    for k in range(1, freq_count):
        inverse = jnp.where(column % freq_count == k, ROTARY_BASE ** (-k / freq_count), inverse)
    angles = spot * inverse
    return (jnp.cos(angles)[:, : ROPE // 2], jnp.sin(angles)[:, : ROPE // 2])


def rotate(vectors, cosine, sine):
    half_width = ROPE // 2
    leading = vectors[:, :half_width]
    trailing = vectors[:, half_width:]
    return [leading * cosine - trailing * sine, leading * sine + trailing * cosine]


def ring_device(place, count):
    return jnp.where(place < count // 2, 2 * place, 2 * (count - 1 - place) + 1)


def ring_place(index, count):
    return jnp.where(index % 2 == 0, index // 2, count - 1 - index // 2)


def dot(left, right):
    return jnp.dot(left, right, preferred_element_type=jnp.float32)


def dot_nt(left, right):
    return lax.dot_general(
        left, right, (((1,), (1,)), ((), ())), preferred_element_type=jnp.float32
    )


def layer_kernel(
    n_sp,
    n_tp,
    splits,
    q_ref,
    lat_ref,
    rope_ref,
    wk_ref,
    wv_ref,
    wo_ref,
    resid_ref,
    gain_mix_ref,
    gain_out_ref,
    wg_ref,
    wu_ref,
    wd_ref,
    out_ref,
    lat_all,
    keys,
    rotary,
    values,
    gate_all,
    up_all,
    down_all,
    q_all,
    heads,
    part_send,
    part_recv,
    stat_send,
    stat_recv,
    rows_all,
    part2_send,
    part2_recv,
    stat2_send,
    stat2_recv,
    hid,
    local_sem,
    lat_send,
    lat_recv,
    share_send,
    share_recv,
    ring_send,
    ring_recv,
    tp_send,
    tp_recv,
    down_send,
    down_recv,
):
    sp = lax.axis_index("sp")
    tp = lax.axis_index("tp")
    place = ring_place(sp, n_sp)
    ahead = ring_device((place + 1) % n_sp, n_sp)
    behind = ring_device((place + n_sp - 1) % n_sp, n_sp)
    targets = (ahead, behind)
    partner = tp + 1 - 2 * (tp % 2)
    core = tp % 2
    n_rows = q_ref.shape[0]
    head_count = wk_ref.shape[1] // NOPE
    rank = wk_ref.shape[0]
    lat_rows = lat_all.shape[2]
    n_cols = out_ref.shape[1]

    barrier = pltpu.get_barrier_semaphore()
    for device in targets:
        pl.semaphore_signal(barrier, inc=1, device_id={"sp": device}, device_id_type=MESH)
    for step in range(1, n_tp):
        pl.semaphore_signal(
            barrier, inc=1, device_id={"tp": (tp + step) % n_tp}, device_id_type=MESH
        )

    own = []
    lat_own = pltpu.make_async_copy(
        lat_ref, lat_all.at[sp, :, :, pl.ds(0, rank)], local_sem.at[0]
    )
    lat_own.start()
    weights = (gate_all, up_all, down_all)
    for i, source in enumerate((wg_ref, wu_ref)):
        copy = pltpu.make_async_copy(source, weights[i].at[sp], local_sem.at[i + 1])
        copy.start()
        own.append(copy)
    cosine, sine = rotary_tables(sp * n_rows, n_rows)
    key_rot = rotate(rope_ref[...].astype(jnp.float32), cosine, sine)
    key_rot.append(jnp.zeros((n_rows, LANES - ROPE), jnp.float32))
    lat_all[sp, :, :, pl.ds(rank, LANES)] = (
        jnp.concatenate(key_rot, axis=1).astype(jnp.bfloat16).reshape(4, lat_rows, LANES)
    )

    def prepare_queries(head):
        base = head * (NOPE + ROPE)
        wide_q = q_ref[...].astype(jnp.float32)
        nope = wide_q[:, base : base + NOPE]
        other = jnp.zeros((n_rows, NOPE), jnp.float32)
        rotary = rotate(wide_q[:, base + NOPE : base + NOPE + ROPE], cosine, sine)
        parts = [nope, other] if head % 2 == 0 else [other, nope]
        parts = parts + rotary + [jnp.zeros((n_rows, LANES - ROPE), jnp.float32)]
        q_all[head] = jnp.concatenate(parts, axis=1).astype(jnp.bfloat16)

    def prepare_down():
        count = wd_ref.shape[1]
        across = lax.broadcasted_iota(jnp.int32, (count, count), 1)
        diagonal = (lax.broadcasted_iota(jnp.int32, (count, count), 0) == across).astype(
            jnp.float32
        ).astype(jnp.bfloat16)
        down_all[sp] = dot_nt(diagonal, wd_ref[...]).astype(jnp.bfloat16)

    preparing = [functools.partial(prepare_queries, head) for head in range(head_count)]
    preparing.append(prepare_down)
    pl.semaphore_wait(barrier, 2 + n_tp - 1)

    def origin(hop, direction):
        if direction == 0:
            return ring_device((place + n_sp - hop) % n_sp, n_sp)
        return ring_device((place + hop) % n_sp, n_sp)

    def lat_copy(hop, direction):
        block = lat_all.at[origin(hop - 1, direction), core * 2 + direction]
        return pltpu.make_async_remote_copy(
            src_ref=block,
            dst_ref=block,
            send_sem=lat_send.at[direction],
            recv_sem=lat_recv.at[direction, hop - 1],
            device_id={"sp": targets[direction]},
            device_id_type=MESH,
        )

    def lat_arrival(hop, direction):
        block = lat_all.at[origin(hop, direction), core * 2 + direction]
        return pltpu.make_async_remote_copy(
            src_ref=block,
            dst_ref=block,
            send_sem=lat_send.at[direction],
            recv_sem=lat_recv.at[direction, hop - 1],
            device_id={"sp": targets[direction]},
            device_id_type=MESH,
        )

    def share_copy(hop, direction, which):
        block = lat_all.at[origin(hop, direction), which * 2 + direction]
        return pltpu.make_async_remote_copy(
            src_ref=block,
            dst_ref=block,
            send_sem=share_send.at[direction],
            recv_sem=share_recv.at[direction, hop - 1],
            device_id={"tp": partner},
            device_id_type=MESH,
        )

    piece_rows = wg_ref.shape[0] // (2 * splits)

    def ring_copy(array, piece, hop, direction, arriving):
        block = origin(hop if arriving else hop - 1, direction)
        rows = pl.ds((direction * splits + piece) * piece_rows, piece_rows)
        ref = weights[array].at[block, rows]
        return pltpu.make_async_remote_copy(
            src_ref=ref,
            dst_ref=ref,
            send_sem=ring_send.at[array, piece, direction],
            recv_sem=ring_recv.at[array, piece, direction, hop - 1],
            device_id={"sp": targets[direction]},
            device_id_type=MESH,
        )

    started = set()

    def ring_step(array, piece, hop):
        if hop == 1 and array < 2 and array not in started:
            own[array].wait()
            started.add(array)
        for direction in range(2):
            if hop > 1:
                ring_copy(array, piece, hop - 1, direction, True).wait_recv()
                ring_copy(array, piece, hop - 1, direction, False).wait_send()
            if hop < n_sp:
                ring_copy(array, piece, hop, direction, False).start()

    first = [
        (array, piece, hop)
        for hop in range(1, n_sp)
        for array in range(2)
        for piece in range(splits)
    ]
    second = [(2, piece, hop) for hop in range(1, n_sp) for piece in range(splits)]
    queue = [first + second, 0]

    def advance(count):
        steps, at = queue
        for step in steps[at : at + count]:
            ring_step(*step)
        queue[1] = min(at + count, len(steps))

    unit = max(1, len(first) // 28)

    lat_own.wait()
    for hop in range(1, n_sp + 1):
        for direction in range(2):
            if hop > 1:
                lat_arrival(hop - 1, direction).wait_recv()
                lat_copy(hop - 1, direction).wait_send()
            if hop < n_sp:
                lat_copy(hop, direction).start()
            if hop > 2:
                share_copy(hop - 2, direction, core).wait_send()
            if hop > 1:
                share_copy(hop - 1, direction, core).start()
        if hop < n_sp and queue[1] < 7 * unit:
            advance(1)
        if preparing:
            preparing.pop(0)()
    while preparing:
        preparing.pop(0)()
    for direction in range(2):
        share_copy(n_sp - 1, direction, core).wait_send()
        for hop in range(1, n_sp):
            share_copy(hop, direction, 1 - core).wait_recv()

    total_rows = n_sp * n_rows
    lat_wide = lat_all.shape[3]
    chunk_blocks = max(1, min(n_sp, 1536 // n_rows))
    chunks = n_sp // chunk_blocks
    chunk = chunk_blocks * n_rows
    half_blocks = max(1, chunk_blocks // 2)

    def project(step):
        rows = half_blocks * n_rows
        blocks = pl.ds(step * half_blocks, half_blocks)
        lat = lat_all[blocks, :, :, pl.ds(0, rank)].reshape(rows, rank)
        rotary[pl.ds(step * rows, rows)] = lat_all[blocks, :, :, pl.ds(rank, LANES)].reshape(
            rows, LANES
        )
        keys[pl.ds(step * rows, rows)] = dot(lat, wk_ref[...]).astype(jnp.bfloat16)
        values[pl.ds(step * rows, rows)] = dot(lat, wv_ref[...]).astype(jnp.bfloat16)

    if chunks == 1:
        for step in range(n_sp // half_blocks):
            project(step)
            advance(unit)
    else:
        pl.loop(0, n_sp // half_blocks)(project)
        advance(2 * unit)

    score_scale = (NOPE + ROPE) ** (-0.5)
    lane = lax.broadcasted_iota(jnp.int32, (n_rows, LANES), 1)

    def attend(head, at, state):
        maxima, totals, running = state
        rows = pl.ds(at * chunk, chunk)
        pair = slice(head // 2 * LANES, (head // 2 + 1) * LANES)
        whole_keys = jnp.concatenate([keys[rows, pair], rotary[rows]], axis=1)
        scores = dot_nt(q_all[head], whole_keys) * score_scale
        top = jnp.max(scores, axis=1, keepdims=True)
        if maxima is not None:
            top = jnp.maximum(maxima, top)
        probs = jnp.exp(scores - top)
        sums = jnp.sum(probs, axis=1, keepdims=True)
        update = dot(probs.astype(jnp.bfloat16), values[rows, pair])
        if maxima is not None:
            factor = jnp.exp(maxima - top)
            sums = totals * factor + sums
            update = running * factor + update
        return (top, sums, update)

    for head in range(head_count):
        state = attend(head, 0, (None, None, None))
        if chunks > 1:
            state = lax.fori_loop(1, chunks, functools.partial(attend_loop, attend, head), state)
        result = state[2] / state[1]
        pair = slice(head // 2 * LANES, (head // 2 + 1) * LANES)
        if head % 2 == 0:
            heads[:, pair] = result.astype(jnp.bfloat16)
        else:
            heads[:, pair] = jnp.where(
                lane < VDIM, heads[:, pair].astype(jnp.float32), result
            ).astype(jnp.bfloat16)
        advance(unit)

    def tp_copy(stage, slot_source, slot_target, to, slot_semaphore):
        return pltpu.make_async_remote_copy(
            src_ref=slot_source,
            dst_ref=slot_target,
            send_sem=tp_send.at[stage, slot_semaphore],
            recv_sem=tp_recv.at[stage, slot_semaphore],
            device_id={"tp": to},
            device_id_type=MESH,
        )

    def exchange(stage, source_of, target_of):
        copies = []
        for k in range(1, n_tp):
            to = (tp + k) % n_tp
            copies.append(tp_copy(stage, source_of(to), target_of(k), to, k))
        return copies

    copies = exchange(0, lambda to: part_send.at[to], lambda k: part_recv.at[k])
    for k in range(1, n_tp + 1):
        to = (tp + k) % n_tp
        part_send[to] = dot(
            heads[...], wo_ref[:, pl.ds(pl.multiple_of(to * n_cols, LANES), n_cols)]
        ).astype(jnp.bfloat16)
        if k < n_tp:
            copies[k - 1].start()
    advance(4 * unit)
    mixed = DEEP_ALPHA * resid_ref[...].astype(jnp.float32) + part_send[tp].astype(jnp.float32)
    for k in range(1, n_tp):
        copies[k - 1].wait_recv()
        mixed = mixed + part_recv[k].astype(jnp.float32)
    pending = list(copies)

    width_total = n_cols * n_tp

    def normed(rows_in, gain_ref, stage, send, recv, between):
        sums = jnp.sum(rows_in, axis=1, keepdims=True)
        squares = jnp.sum(rows_in * rows_in, axis=1, keepdims=True)
        mine = jnp.transpose(jnp.where(lane < 4, sums, squares))[:8]
        send[...] = mine
        copies = exchange(stage, lambda to: send, lambda k: recv.at[k])
        for copy in copies:
            copy.start()
        between()
        for k in range(1, n_tp):
            copies[k - 1].wait_recv()
            mine = mine + recv[k]
        pending.extend(copies)
        whole = jnp.transpose(mine) / width_total
        row_mean = whole[:, :1]
        variance = whole[:, 4:5] - row_mean * row_mean
        return (
            (rows_in - row_mean) * lax.rsqrt(variance + NORM_EPSILON) * gain_ref[...]
        ).astype(jnp.bfloat16)

    hidden_in = normed(
        mixed, gain_mix_ref, 1, stat_send, stat_recv, lambda: advance(2 * unit)
    )
    rows_all[tp] = hidden_in
    copies = exchange(2, lambda to: rows_all.at[tp], lambda k: rows_all.at[tp])
    for copy in copies:
        copy.start()
    pending.extend(copies)
    advance(4 * unit)
    for k in range(1, n_tp):
        sender = (tp + n_tp - k) % n_tp
        tp_copy(2, rows_all.at[sender], rows_all.at[sender], sender, k).wait_recv()

    advance(len(first) - queue[1])
    advance(splits)

    def last_hop(array):
        for piece in range(splits):
            for direction in range(2):
                ring_copy(array, piece, n_sp - 1, direction, True).wait_recv()
                ring_copy(array, piece, n_sp - 1, direction, False).wait_send()

    last_hop(0)
    group = n_sp // n_tp
    depth = group * wg_ref.shape[0]
    hidden_width = wg_ref.shape[1]

    def wide(weight):
        total = None
        for t in range(n_tp):
            term = dot(
                rows_all[t],
                weight[t * group : (t + 1) * group].reshape(depth, hidden_width),
            )
            total = term if total is None else total + term
            advance(1)
        return total

    gate_sum = wide(gate_all)
    last_hop(1)
    up_sum = wide(up_all)
    hidden = (gate_sum / (1.0 + jnp.exp(-gate_sum)) * up_sum).astype(jnp.bfloat16)
    advance(1)

    half_rows = piece_rows * splits
    if half_rows % LANES == 0:
        hid[...] = hidden

        def down_copy(k, slot, to, columns):
            ref = part2_send.at[to, :, columns]
            return pltpu.make_async_remote_copy(
                src_ref=ref,
                dst_ref=part2_recv.at[k, :, columns],
                send_sem=down_send.at[k, slot],
                recv_sem=down_recv.at[k, slot],
                device_id={"tp": to},
                device_id_type=MESH,
            )

        def slot_columns(slot):
            return pl.ds(pl.multiple_of(slot * half_rows, LANES), half_rows)

        def make_columns(hop):
            for direction in range(2):
                block = origin(hop, direction)
                owner = block // group
                slot = (block % group) * 2 + direction
                rows = pl.ds(direction * half_rows, half_rows)
                part2_send[owner, :, slot_columns(slot)] = dot_nt(
                    hid[...], down_all[block, rows]
                ).astype(jnp.bfloat16)

                @pl.when(owner != tp)
                def send_away():
                    down_copy((owner + n_tp - tp) % n_tp, slot, owner, slot_columns(slot)).start()

        made = 0
        while queue[1] < len(queue[0]):
            array, piece, hop = queue[0][queue[1]]
            advance(1)
            if piece == splits - 1:
                made_to = hop
                while made < made_to:
                    make_columns(made)
                    made += 1
        while made < n_sp - 1:
            make_columns(made)
            made += 1
        last_hop(2)
        make_columns(n_sp - 1)
        mixer = part2_send[tp].astype(jnp.float32)
        for k in range(1, n_tp):
            for slot in range(2 * group):
                down_copy(k, slot, (tp + k) % n_tp, slot_columns(slot)).wait_recv()
            mixer = mixer + part2_recv[k].astype(jnp.float32)
    else:
        advance(len(queue[0]))
        last_hop(2)
        copies = exchange(3, lambda to: part2_send.at[to], lambda k: part2_recv.at[k])
        for k in range(1, n_tp + 1):
            to = (tp + k) % n_tp
            part2_send[to] = dot_nt(
                hidden, down_all[pl.ds(to * group, group)].reshape(depth, hidden_width)
            ).astype(jnp.bfloat16)
            if k < n_tp:
                copies[k - 1].start()
        mixer = part2_send[tp].astype(jnp.float32)
        for k in range(1, n_tp):
            copies[k - 1].wait_recv()
            mixer = mixer + part2_recv[k].astype(jnp.float32)
        pending.extend(copies)
    final = DEEP_ALPHA * rows_all[tp].astype(jnp.float32) + HALF_STEP * mixer
    out_ref[...] = normed(final, gain_out_ref, 4, stat2_send, stat2_recv, lambda: None)
    for copy in pending:
        copy.wait_send()
    if half_rows % LANES == 0:
        for k in range(1, n_tp):
            for slot in range(2 * group):
                down_copy(k, slot, (tp + k) % n_tp, slot_columns(slot)).wait_send()


def attend_loop(attend, head, at, state):
    return attend(head, at, state)


def local(
    queries,
    latents,
    rope_key,
    w_key,
    w_value,
    w_out,
    resid,
    gain_mix,
    w_gate,
    w_up,
    w_down,
    gain_out,
):
    n_sp = lax.axis_size("sp")
    n_tp = lax.axis_size("tp")
    rows = queries.shape[0]
    head_count = w_key.shape[1] // NOPE
    rank = latents.shape[1]
    cols = resid.shape[1]
    hidden_width = w_gate.shape[1]
    weight_rows = w_gate.shape[0]
    lat_wide = rank + LANES
    splits = 2 if weight_rows % 64 == 0 else 1
    bf16 = jnp.bfloat16
    total_rows = n_sp * rows
    vmem = pl.BlockSpec(memory_space=pltpu.VMEM)
    anywhere = pl.BlockSpec(memory_space=pl.ANY)
    dma = pltpu.SemaphoreType.DMA
    return pl.pallas_call(
        functools.partial(layer_kernel, n_sp, n_tp, splits),
        out_shape=jax.ShapeDtypeStruct((rows, cols), bf16),
        in_specs=[vmem, anywhere] + [vmem] * 7 + [anywhere] * 2 + [vmem],
        out_specs=vmem,
        scratch_shapes=[
            pltpu.VMEM((n_sp, 4, rows // 4, lat_wide), bf16),
            pltpu.VMEM((total_rows, head_count * NOPE), bf16),
            pltpu.VMEM((total_rows, LANES), bf16),
            pltpu.VMEM((total_rows, head_count * VDIM), bf16),
            pltpu.VMEM((n_sp, weight_rows, hidden_width), bf16),
            pltpu.VMEM((n_sp, weight_rows, hidden_width), bf16),
            pltpu.VMEM((n_sp, weight_rows, hidden_width), bf16),
            pltpu.VMEM((head_count, rows, 2 * LANES), bf16),
            pltpu.VMEM((rows, head_count * VDIM), bf16),
            pltpu.VMEM((n_tp, rows, cols), bf16),
            pltpu.VMEM((n_tp, rows, cols), bf16),
            pltpu.VMEM((8, rows), jnp.float32),
            pltpu.VMEM((n_tp, 8, rows), jnp.float32),
            pltpu.VMEM((n_tp, rows, cols), bf16),
            pltpu.VMEM((n_tp, rows, cols), bf16),
            pltpu.VMEM((n_tp, rows, cols), bf16),
            pltpu.VMEM((8, rows), jnp.float32),
            pltpu.VMEM((n_tp, 8, rows), jnp.float32),
            pltpu.VMEM((rows, hidden_width), bf16),
            dma((4,)),
            dma((2,)),
            dma((2, n_sp - 1)),
            dma((2,)),
            dma((2, n_sp - 1)),
            dma((3, splits, 2)),
            dma((3, splits, 2, n_sp - 1)),
            dma((5, n_tp)),
            dma((5, n_tp)),
            dma((n_tp, 2 * (n_sp // n_tp))),
            dma((n_tp, 2 * (n_sp // n_tp))),
        ],
        compiler_params=pltpu.CompilerParams(
            collective_id=0, has_side_effects=True, vmem_limit_bytes=66000000
        ),
    )(
        queries,
        latents.reshape(4, rows // 4, rank),
        rope_key,
        w_key,
        w_value,
        w_out,
        resid,
        gain_mix.reshape(1, -1),
        gain_out.reshape(1, -1),
        w_gate,
        w_up,
        w_down,
    )


def solution(mesh):
    placed = (
        P("sp", "tp"),
        P("sp", None),
        P("sp", None),
        P(None, "tp"),
        P(None, "tp"),
        P("tp", None),
        P("sp", "tp"),
        P("tp"),
        P("sp", "tp"),
        P("sp", "tp"),
        P("tp", "sp"),
        P("tp"),
    )
    return jax.shard_map(
        local, mesh=mesh, in_specs=placed, out_specs=P("sp", "tp"), check_vma=False
    )
```

profile of v0, /device:TPU:0, one launch (start us, length us, event | category | flops | bytes accessed | tf_op | source)
XLA Modules:
  0.0 122.8 jit_solution(12947884380134890903)
XLA Ops:
  0.0 1.4 %copy.13.rope_ref = bf16[192,32]{1,0:T(8,128)(2,1)} copy(bf16[192,32]{0,1:T(8,128)(2,1)} %param.14) | data formatting | bytes 24576 | tf_op args[2]
  1.4 119.7 %shard_map.118 = bf16[192,512]{1,0:T(8,128)(2,1)} custom-call(bf16[192,384]{1,0:T(8,128)(2,1)} %q_ref.1, bf16[4,48,512]{2,1,0:T(8,128)(2,1)} %bitcast.3, bf16[192,32]{1,0:T(8,128)(2,1)} %copy.13.rope_ref, bf16[512,256]{1,0:T(8,128)(2,1)} %wk_ref.1, bf16[512,256]{1,0:T(8,128)(2,1)} %wv_ref.1, bf16[256,2048]{1,0:T(8,128)(2,1)} %wo_ref.1, ...), custom_call_target="tpu_custom_call" | custom-call | tf_op jit(solution)/shard_map/pallas_call | solution.py:545
  121.2 1.6 %copy.15 = bf16[192,512]{1,0:T(8,128)(2,1)} copy(bf16[192,512]{1,0:T(8,128)(2,1)} %shard_map.118) | data formatting | bytes 393216
where the time goes:
time: 123 us
  Pallas kernels  120 us (98%)
  local copies, waits for them, and re-layouts  3.05 us (2%)
    pallas_call x1, Pallas kernels, local(): pl.pallas_call(functools.partial(layer_kernel, n_sp, n_tp, splits), out_s...  120 us
    unnamed x2, local copies, waits for them, and re-layouts  3.05 us

commit v1 on v0

--- a/solution.py
+++ b/solution.py
@@ -513,6 +513,716 @@
     return attend(head, at, state)
 
 
+def flip(value, mask):
+    result = value
+    bit = 1
+    while bit <= mask:
+        if mask & bit:
+            result = result + bit - 2 * bit * ((value // bit) % 2)
+        bit *= 2
+    return result
+
+
+class Slots:
+    def __init__(self, sends, recvs):
+        self.sends, self.recvs, self.base, self.used = sends, recvs, {}, 0
+
+    def at(self, name, count, index):
+        if name not in self.base:
+            self.base[name] = self.used
+            self.used += count
+        place = self.base[name] + index
+        return self.sends.at[place], self.recvs.at[place]
+
+
+def slot_total(n_hi, pieces):
+    return 16 * n_hi + 6 * n_hi * pieces + 64
+
+
+def paired_kernel(
+    n_sp,
+    n_tp,
+    pieces,
+    q_in,
+    lat_ref,
+    rope_in,
+    wk_in,
+    wv_in,
+    wo_ref,
+    resid_in,
+    gain_mix_in,
+    gain_out_in,
+    wg_ref,
+    wu_ref,
+    wd_ref,
+    out_ref,
+    q_ref,
+    rope_ref,
+    wk_ref,
+    wv_ref,
+    resid_ref,
+    gain_mix_ref,
+    gain_out_ref,
+    lat_all,
+    keys,
+    rotary,
+    values,
+    q_all,
+    heads_all,
+    wo_all,
+    wide_all,
+    down_all,
+    rows_all,
+    hid,
+    summed,
+    core_send,
+    core_recv,
+    far_send,
+    far_recv,
+    pair_send,
+    pair_recv,
+    stat_send,
+    stat_recv,
+    local_sem,
+    input_sem,
+    sends,
+    recvs,
+):
+    sp = lax.axis_index("sp")
+    tp = lax.axis_index("tp")
+    n_hi = n_sp // 2
+    z, x = sp // 2, sp % 2
+    half = z % 2
+    edge = half == (z // 2) % 2
+    n_rows = q_ref.shape[0]
+    head_count = wk_ref.shape[1] // NOPE
+    rank = wk_ref.shape[0]
+    lat_rows = lat_all.shape[2]
+    n_cols = out_ref.shape[1]
+    group = n_sp // n_tp
+    depth = wg_ref.shape[0]
+    width = wg_ref.shape[1] // 2
+    down_cols = wd_ref.shape[1]
+    total_rows = n_sp * n_rows
+    slots = Slots(sends, recvs)
+    pending = []
+
+    order = [(1, flip(z, 1))]
+    for m in range(2, n_hi, 2):
+        low, high = flip(z, m), flip(z, m + 1)
+        order.append((jnp.where(edge, m, m + 1), jnp.where(edge, low, high)))
+        order.append((jnp.where(edge, m + 1, m), jnp.where(edge, high, low)))
+
+    def sp_of(place, side):
+        return 2 * place + side
+
+    def remote(name, count, index, source, target, device):
+        send, recv = slots.at(name, count, index)
+        return pltpu.make_async_remote_copy(
+            src_ref=source,
+            dst_ref=target,
+            send_sem=send,
+            recv_sem=recv,
+            device_id=device,
+            device_id_type=MESH,
+        )
+
+    def start(copy):
+        copy.start()
+        pending.append(copy)
+
+    other_x = 1 - x
+    partner, across, corner = flip(tp, 1), flip(tp, 2), flip(tp, 3)
+    to_x = {"sp": sp_of(z, other_x)}
+    to_pair = {"sp": sp_of(flip(z, 1), x)}
+    to_core = {"tp": partner}
+    to_across = {"tp": across}
+
+    barrier = pltpu.get_barrier_semaphore()
+    peers = [{"sp": sp_of(flip(z, k), x)} for k in range(1, n_hi)] + [to_x]
+    peers += [{"tp": flip(tp, j)} for j in range(1, n_tp)]
+    peers.append({"sp": sp_of(flip(z, 1), x), "tp": across})
+    for device in peers:
+        pl.semaphore_signal(barrier, inc=1, device_id=device, device_id_type=MESH)
+
+    inputs = {}
+    for at, (name, source, target) in enumerate(
+        (
+            ("rope", rope_in, rope_ref),
+            ("q", q_in, q_ref),
+            ("wk", wk_in, wk_ref),
+            ("wv", wv_in, wv_ref),
+            ("resid", resid_in, resid_ref),
+            ("mix", gain_mix_in, gain_mix_ref),
+            ("out", gain_out_in, gain_out_ref),
+        )
+    ):
+        inputs[name] = pltpu.make_async_copy(source, target, input_sem.at[at])
+
+    def weight_rows(array, piece):
+        size = (depth if array < 2 else width) // pieces
+        return piece * size, size
+
+    def weight_source(array, which, piece):
+        first, size = weight_rows(array, piece)
+        if array == 2:
+            return wd_ref.at[pl.ds(pl.multiple_of(which * width + first, 16), size)]
+        columns = pl.ds(pl.multiple_of(which * width, LANES), width)
+        return (wg_ref, wu_ref)[array].at[pl.ds(first, size), columns]
+
+    def weight_block(array, block, piece):
+        first, size = weight_rows(array, piece)
+        if array == 2:
+            return down_all.at[block, pl.ds(first, size)]
+        return wide_all.at[block, pl.ds(first, size), pl.ds(array * width, width)]
+
+    def weight_out(array, k):
+        place = flip(z, k)
+        for piece in range(pieces):
+            remote(
+                ("wz", array, piece),
+                n_hi,
+                k,
+                weight_source(array, place % 2, piece),
+                weight_block(array, sp, piece),
+                {"sp": sp_of(place, x)},
+            ).start()
+
+    def weight_in(array, at, piece):
+        k, place = order[at]
+        block = weight_block(array, sp_of(place, x), piece)
+        return remote(("wz", array, piece), n_hi, k, block, block, to_x)
+
+    def weight_side(array, k, place, piece):
+        block = weight_block(array, sp_of(place, x), piece)
+        return remote(("wx", array, piece), n_hi, k, block, block, to_x)
+
+    def weight_side_in(array, k, place, piece):
+        block = weight_block(array, sp_of(place, other_x), piece)
+        return remote(("wx", array, piece), n_hi, k, block, block, to_x)
+
+    def weight_own(array, piece):
+        start(
+            remote(
+                ("wx", array, piece),
+                n_hi,
+                0,
+                weight_source(array, half, piece),
+                weight_block(array, sp, piece),
+                to_x,
+            )
+        )
+
+    def relay(array, at):
+        for piece in range(pieces):
+            weight_in(array, at, piece).wait_recv()
+            start(weight_side(array, order[at][0], order[at][1], piece))
+
+    lat_own = pltpu.make_async_copy(
+        lat_ref, lat_all.at[sp, :, :, pl.ds(0, rank)], local_sem.at[0]
+    )
+    inputs["rope"].start()
+    lat_own.start()
+    for name in ("q", "wk", "wv", "resid", "mix", "out"):
+        inputs[name].start()
+    own = []
+    for array in range(3):
+        for piece in range(pieces):
+            copy = pltpu.make_async_copy(
+                weight_source(array, half, piece),
+                weight_block(array, sp, piece),
+                local_sem.at[1 + array * pieces + piece],
+            )
+            copy.start()
+            own.append(copy)
+
+    def wo_columns(which):
+        return wo_ref.at[:, pl.ds(pl.multiple_of(which * n_cols, LANES), n_cols)]
+
+    wo_own = pltpu.make_async_copy(
+        wo_columns(tp), wo_all.at[tp], local_sem.at[1 + 3 * pieces]
+    )
+    wo_own.start()
+    cosine, sine = rotary_tables(sp * n_rows, n_rows)
+    inputs["rope"].wait()
+    turned_in = jnp.concatenate(
+        [rope_ref[...].astype(jnp.float32), jnp.zeros((LANES - ROPE, n_rows), jnp.float32)],
+        axis=0,
+    )
+    key_rot = rotate(jnp.transpose(turned_in)[:, :ROPE], cosine, sine)
+    key_rot.append(jnp.zeros((n_rows, LANES - ROPE), jnp.float32))
+    lat_all[sp, :, :, pl.ds(rank, LANES)] = (
+        jnp.concatenate(key_rot, axis=1).astype(jnp.bfloat16).reshape(n_tp, lat_rows, LANES)
+    )
+
+    def prepare_queries(head):
+        base = head * (NOPE + ROPE)
+        wide_q = q_ref[...].astype(jnp.float32)
+        nope = wide_q[:, base : base + NOPE]
+        other = jnp.zeros((n_rows, NOPE), jnp.float32)
+        turned = rotate(wide_q[:, base + NOPE : base + NOPE + ROPE], cosine, sine)
+        parts = [nope, other] if head % 2 == 0 else [other, nope]
+        parts = parts + turned + [jnp.zeros((n_rows, LANES - ROPE), jnp.float32)]
+        q_all[head] = jnp.concatenate(parts, axis=1).astype(jnp.bfloat16)
+
+    pl.semaphore_wait(barrier, len(peers))
+    lat_own.wait()
+
+    def lat_block(place, side, quarter):
+        return lat_all.at[sp_of(place, side), quarter]
+
+    def lat_copy(name, k, place, side, quarter, device):
+        block = lat_block(place, side, quarter)
+        return remote(("lat", name), n_hi, k, block, block, device)
+
+    def lat_z_in(at):
+        k, place = order[at]
+        lat_copy("z", k, place, x, tp, to_x).wait_recv()
+        start(lat_copy("x", k, place, x, tp, to_x))
+        start(lat_copy("y", k, place, x, tp, to_across))
+        start(lat_copy("cz", k, place, x, tp, to_core))
+
+    def lat_x_in(k, place):
+        lat_copy("x", k, place, other_x, tp, to_x).wait_recv()
+        start(lat_copy("yd", k, place, other_x, tp, to_across))
+        start(lat_copy("cx", k, place, other_x, tp, to_core))
+
+    def lat_y_in(k, place):
+        lat_copy("y", k, place, x, across, to_across).wait_recv()
+        start(lat_copy("cy", k, place, x, across, to_core))
+
+    def lat_yd_in(k, place):
+        lat_copy("yd", k, place, other_x, across, to_across).wait_recv()
+        start(lat_copy("cyd", k, place, other_x, across, to_core))
+
+    for k in list(range(n_hi - 1, 0, -1)):
+        block = lat_block(z, x, tp)
+        start(remote(("lat", "z"), n_hi, k, block, block, {"sp": sp_of(flip(z, k), x)}))
+    start(lat_copy("x", 0, z, x, tp, to_x))
+    weight_own(0, 0)
+
+    far = list(range(2, n_hi))
+
+    def first_batch():
+        for array in range(3):
+            weight_out(array, 1)
+        for array in range(2):
+            for k in far:
+                weight_out(array, k)
+
+    def second_batch():
+        for k in far:
+            weight_out(2, k)
+
+    @pl.when(edge)
+    def outer_first():
+        first_batch()
+
+    inputs["q"].wait()
+    prepare_queries(0)
+    lat_x_in(0, z)
+    lat_z_in(0)
+
+    @pl.when(jnp.logical_not(edge))
+    def inner_first():
+        first_batch()
+
+    prepare_queries(1)
+    lat_z_in(1)
+    lat_x_in(*order[0])
+    for at in range(2, len(order)):
+        lat_z_in(at)
+    for head in range(2, head_count):
+        prepare_queries(head)
+    for at in range(1, len(order)):
+        lat_x_in(*order[at])
+    lat_y_in(*order[0])
+    lat_yd_in(0, z)
+    lat_yd_in(*order[0])
+    for at in range(1, len(order)):
+        lat_y_in(*order[at])
+    for piece in range(1, pieces):
+        weight_own(0, piece)
+    for array in (1, 2):
+        for piece in range(pieces):
+            weight_own(array, piece)
+    for j in (2, 3, 1):
+        to = flip(tp, j)
+        start(
+            remote("wo", n_tp, j, wo_columns(to), wo_all.at[tp], {"tp": to})
+        )
+    for at in range(1, len(order)):
+        lat_yd_in(*order[at])
+    for k, place in [(0, z)] + order:
+        if place is not z:
+            lat_copy("cz", k, place, x, partner, to_core).wait_recv()
+            lat_copy("cy", k, place, x, corner, to_core).wait_recv()
+        lat_copy("cx", k, place, other_x, partner, to_core).wait_recv()
+        lat_copy("cyd", k, place, other_x, corner, to_core).wait_recv()
+
+    near, rest = list(range(1, len(order), 2)), list(range(2, len(order), 2))
+    relays = [(0, 0)] + [(0, at) for at in near] + [(1, 0), (2, 0)]
+    relays += [(1, at) for at in near] + [(0, at) for at in rest]
+    relays_early = len(relays)
+    relays += [(1, at) for at in rest]
+    relays_wide = len(relays)
+    relays += [(2, at) for at in near] + [(2, at) for at in rest]
+    queue = [0]
+
+    def advance(count):
+        for array, at in relays[queue[0] : queue[0] + count]:
+            relay(array, at)
+        queue[0] = min(queue[0] + count, len(relays))
+
+    half_blocks = n_sp // 2
+
+    def project(step):
+        rows = half_blocks * n_rows
+        blocks = pl.ds(step * half_blocks, half_blocks)
+        lat = lat_all[blocks, :, :, pl.ds(0, rank)].reshape(rows, rank)
+        rotary[pl.ds(step * rows, rows)] = lat_all[blocks, :, :, pl.ds(rank, LANES)].reshape(
+            rows, LANES
+        )
+        keys[pl.ds(step * rows, rows)] = dot(lat, wk_ref[...]).astype(jnp.bfloat16)
+        values[pl.ds(step * rows, rows)] = dot(lat, wv_ref[...]).astype(jnp.bfloat16)
+
+    inputs["wk"].wait()
+    inputs["wv"].wait()
+    advance(1)
+    for step in range(n_sp // half_blocks):
+        project(step)
+    advance(1)
+
+    score_scale = (NOPE + ROPE) ** (-0.5)
+    lane = lax.broadcasted_iota(jnp.int32, (n_rows, LANES), 1)
+
+    def heads_copy(piece, j, owner):
+        block = heads_all.at[owner, :, pl.ds(piece * LANES, LANES)]
+        return remote(("heads", piece), n_tp, j, block, block, {"tp": flip(tp, j)})
+
+    for head in range(head_count):
+        pair = slice(head // 2 * LANES, (head // 2 + 1) * LANES)
+        whole_keys = jnp.concatenate([keys[:, pair], rotary[...]], axis=1)
+        scores = dot_nt(q_all[head], whole_keys) * score_scale
+        top = jnp.max(scores, axis=1, keepdims=True)
+        probs = jnp.exp(scores - top)
+        sums = jnp.sum(probs, axis=1, keepdims=True)
+        result = dot(probs.astype(jnp.bfloat16), values[:, pair]) / sums
+        if head % 2 == 0:
+            held = result
+        else:
+            heads_all[tp, :, pair] = jnp.where(lane < VDIM, held, result).astype(jnp.bfloat16)
+            for j in (2, 3, 1):
+                start(heads_copy(head // 2, j, tp))
+        if head < head_count - 1:
+            advance(1)
+
+    @pl.when(jnp.logical_not(edge))
+    def inner_rest():
+        second_batch()
+
+    advance(relays_early - queue[0])
+    inputs["resid"].wait()
+    inputs["mix"].wait()
+    inputs["out"].wait()
+    mixed = DEEP_ALPHA * resid_ref[...].astype(jnp.float32)
+    wo_own.wait()
+    mixed = mixed + dot(heads_all[tp], wo_all[tp])
+    for j in (1, 2, 3):
+        sender = flip(tp, j)
+        remote("wo", n_tp, j, wo_all.at[sender], wo_all.at[sender], to_core).wait_recv()
+        for piece in range(head_count // 2):
+            heads_copy(piece, j, sender).wait_recv()
+        mixed = mixed + dot(heads_all[sender], wo_all[sender])
+
+    width_total = n_cols * n_tp
+
+    def normed(rows_in, gain_ref, stage, between):
+        sums = jnp.sum(rows_in, axis=1, keepdims=True)
+        squares = jnp.sum(rows_in * rows_in, axis=1, keepdims=True)
+        mine = jnp.transpose(jnp.where(lane < 4, sums, squares))[:8]
+        stat_send[stage] = mine
+        for j in (2, 3, 1):
+            start(
+                remote(
+                    ("stat", stage),
+                    n_tp,
+                    j,
+                    stat_send.at[stage],
+                    stat_recv.at[stage, j],
+                    {"tp": flip(tp, j)},
+                )
+            )
+        between()
+        for j in (1, 2, 3):
+            remote(
+                ("stat", stage),
+                n_tp,
+                j,
+                stat_send.at[stage],
+                stat_recv.at[stage, j],
+                to_core,
+            ).wait_recv()
+            mine = mine + stat_recv[stage, j]
+        whole = jnp.transpose(mine) / width_total
+        row_mean = whole[:, :1]
+        variance = whole[:, 4:5] - row_mean * row_mean
+        return (
+            (rows_in - row_mean) * lax.rsqrt(variance + NORM_EPSILON) * gain_ref[...]
+        ).astype(jnp.bfloat16)
+
+    hidden_in = normed(mixed, gain_mix_ref, 0, lambda: None)
+    mine = pl.ds(pl.multiple_of(half * n_rows, 16), n_rows)
+    theirs = pl.ds(pl.multiple_of((1 - half) * n_rows, 16), n_rows)
+    rows_all[tp, mine] = hidden_in
+
+    def rows_copy(name, owner, rows, device):
+        block = rows_all.at[owner, rows]
+        return remote(("rows", name), 1, 0, block, block, device)
+
+    start(
+        rows_copy("yz", tp, mine, {"sp": sp_of(flip(z, 1), x), "tp": across})
+    )
+    start(rows_copy("y", tp, mine, to_across))
+    start(rows_copy("z", tp, mine, to_pair))
+    start(rows_copy("c", tp, mine, to_core))
+
+    @pl.when(edge)
+    def outer_rest():
+        second_batch()
+
+    rows_copy("z", tp, theirs, to_pair).wait_recv()
+    start(rows_copy("cz", tp, theirs, to_core))
+    rows_copy("y", across, mine, to_across).wait_recv()
+    start(rows_copy("cy", across, mine, to_core))
+    rows_copy("yz", across, theirs, to_across).wait_recv()
+    start(rows_copy("cyz", across, theirs, to_core))
+    rows_copy("c", partner, mine, to_core).wait_recv()
+    rows_copy("cz", partner, theirs, to_core).wait_recv()
+    rows_copy("cy", corner, mine, to_core).wait_recv()
+    rows_copy("cyz", corner, theirs, to_core).wait_recv()
+    advance(relays_wide - queue[0])
+    for copy in own:
+        copy.wait()
+    for k, place in [(0, z)] + order:
+        for array in range(2):
+            for piece in range(pieces):
+                weight_side_in(array, k, place, piece).wait_recv()
+
+    total = None
+    for t in range(n_tp):
+        term = dot(
+            rows_all[t], wide_all[t * group : (t + 1) * group].reshape(group * depth, 2 * width)
+        )
+        total = term if total is None else total + term
+    gate_sum, up_sum = total[:, :width], total[:, width:]
+    hid[...] = (gate_sum / (1.0 + jnp.exp(-gate_sum)) * up_sum).astype(jnp.bfloat16)
+
+    blocks = []
+    for k, place in [(0, z)] + order:
+        blocks += [(k, place, x), (k, place, other_x)]
+
+    def block_facts(at):
+        k, place, side = blocks[at]
+        block = sp_of(place, side)
+        owner = block // group
+        return block, owner, tp % 2 == owner % 2, tp // 2 == owner // 2
+
+    def core_copy(block):
+        return remote(
+            "core", n_sp, block, core_send.at[block], core_recv.at[block], to_core
+        )
+
+    def far_copy(block):
+        return remote("far", n_sp, block, far_send.at[block], far_recv.at[block], to_across)
+
+    def pair_copy(block):
+        slot = block % group
+        return remote("pair", group, slot, pair_send.at[slot], pair_recv.at[slot], to_pair)
+
+    def make_block(at):
+        block, owner, same_core, same_chip = block_facts(at)
+        product = dot(hid[...], down_all[block])
+
+        @pl.when(same_core)
+        def keep():
+            summed[block] = product
+
+        @pl.when(jnp.logical_not(same_core))
+        def give():
+            core_send[block] = product.astype(jnp.bfloat16)
+            core_copy(block).start()
+
+    def add_core(at):
+        block, owner, same_core, same_chip = block_facts(at)
+
+        @pl.when(same_core)
+        def add():
+            core_copy(block).wait_recv()
+            both = summed[block] + core_recv[block].astype(jnp.float32)
+
+            @pl.when(same_chip)
+            def keep():
+                summed[block] = both
+
+            @pl.when(jnp.logical_not(same_chip))
+            def give():
+                far_send[block] = both.astype(jnp.bfloat16)
+                far_copy(block).start()
+
+    def add_far(at):
+        block, owner, same_core, same_chip = block_facts(at)
+
+        @pl.when(owner == tp)
+        def add():
+            far_copy(block).wait_recv()
+            summed[block] = summed[block] + far_recv[block].astype(jnp.float32)
+            pair_send[block % group] = summed[block, theirs].astype(jnp.bfloat16)
+            pair_copy(block).start()
+
+    def down_ready(at):
+        k, place, side = blocks[at]
+        if at % 2 == 1:
+            for piece in range(pieces):
+                weight_side_in(2, k, place, piece).wait_recv()
+
+    last = len(blocks)
+    steps = last // 2
+    for step in range(steps + 2):
+        if step < steps:
+            if step > 1:
+                advance(1)
+            for at in (2 * step, 2 * step + 1):
+                down_ready(at)
+                make_block(at)
+        if 1 <= step <= steps:
+            add_core(2 * step - 2)
+            add_core(2 * step - 1)
+        if step >= 2:
+            add_far(2 * step - 4)
+            add_far(2 * step - 3)
+
+    final = []
+    for slot in range(group):
+        block = tp * group + slot
+        pair_copy(block).wait_recv()
+        final.append(summed[block, mine] + pair_recv[slot].astype(jnp.float32))
+    mixer = jnp.concatenate(final, axis=1)
+    last_in = DEEP_ALPHA * rows_all[tp, mine].astype(jnp.float32) + HALF_STEP * mixer
+    out_ref[...] = normed(last_in, gain_out_ref, 1, lambda: None)
+
+    for copy in pending:
+        copy.wait_send()
+    for array in range(3):
+        for k in range(1, n_hi):
+            for piece in range(pieces):
+                block = weight_block(array, sp, piece)
+                remote(("wz", array, piece), n_hi, k, block, block, to_x).wait_send()
+    for at in range(last):
+        block, owner, same_core, same_chip = block_facts(at)
+
+        @pl.when(jnp.logical_not(same_core))
+        def core_sent():
+            core_copy(block).wait_send()
+
+        @pl.when(jnp.logical_and(same_core, jnp.logical_not(same_chip)))
+        def far_sent():
+            far_copy(block).wait_send()
+
+    for slot in range(group):
+        pair_copy(tp * group + slot).wait_send()
+
+
+def paired_call(n_sp, n_tp, operands):
+    queries, latents, rope_key, w_key, w_value, w_out, resid, gain_mix = operands[:8]
+    w_gate, w_up, w_down, gain_out = operands[8:]
+    rows = queries.shape[0]
+    head_count = w_key.shape[1] // NOPE
+    rank = latents.shape[1]
+    cols = resid.shape[1]
+    depth, hidden_width = w_gate.shape
+    width = hidden_width // 2
+    down_cols = w_down.shape[1]
+    total_rows = n_sp * rows
+    group = n_sp // n_tp
+    pieces = 2
+    bf16 = jnp.bfloat16
+    vmem = pl.BlockSpec(memory_space=pltpu.VMEM)
+    anywhere = pl.BlockSpec(memory_space=pl.ANY)
+    dma = pltpu.SemaphoreType.DMA
+    count = 132
+    return pl.pallas_call(
+        functools.partial(paired_kernel, n_sp, n_tp, pieces),
+        out_shape=jax.ShapeDtypeStruct((rows, cols), bf16),
+        in_specs=[anywhere] * 12,
+        out_specs=vmem,
+        scratch_shapes=[
+            pltpu.VMEM(queries.shape, bf16),
+            pltpu.VMEM((rope_key.shape[1], rows), bf16),
+            pltpu.VMEM(w_key.shape, bf16),
+            pltpu.VMEM(w_value.shape, bf16),
+            pltpu.VMEM(resid.shape, bf16),
+            pltpu.VMEM((1, cols), jnp.float32),
+            pltpu.VMEM((1, cols), jnp.float32),
+            pltpu.VMEM((n_sp, n_tp, rows // n_tp, rank + LANES), bf16),
+            pltpu.VMEM((total_rows, head_count * NOPE), bf16),
+            pltpu.VMEM((total_rows, LANES), bf16),
+            pltpu.VMEM((total_rows, head_count * VDIM), bf16),
+            pltpu.VMEM((head_count, rows, 2 * LANES), bf16),
+            pltpu.VMEM((n_tp, rows, head_count * VDIM), bf16),
+            pltpu.VMEM((n_tp, head_count * VDIM, cols), bf16),
+            pltpu.VMEM((n_sp, depth, 2 * width), bf16),
+            pltpu.VMEM((n_sp, width, down_cols), bf16),
+            pltpu.VMEM((n_tp, 2 * rows, cols), bf16),
+            pltpu.VMEM((2 * rows, width), bf16),
+            pltpu.VMEM((n_sp, 2 * rows, down_cols), jnp.float32),
+            pltpu.VMEM((n_sp, 2 * rows, down_cols), bf16),
+            pltpu.VMEM((n_sp, 2 * rows, down_cols), bf16),
+            pltpu.VMEM((n_sp, 2 * rows, down_cols), bf16),
+            pltpu.VMEM((n_sp, 2 * rows, down_cols), bf16),
+            pltpu.VMEM((group, rows, down_cols), bf16),
+            pltpu.VMEM((group, rows, down_cols), bf16),
+            pltpu.VMEM((2, 8, rows), jnp.float32),
+            pltpu.VMEM((2, n_tp, 8, rows), jnp.float32),
+            dma((2 + 3 * pieces,)),
+            dma((7,)),
+            dma((count,)),
+            dma((count,)),
+        ],
+        compiler_params=pltpu.CompilerParams(
+            collective_id=1, has_side_effects=True, vmem_limit_bytes=66000000
+        ),
+    )(
+        queries,
+        latents.reshape(n_tp, rows // n_tp, rank),
+        rope_key.T,
+        w_key,
+        w_value,
+        w_out,
+        resid,
+        gain_mix.reshape(1, -1),
+        gain_out.reshape(1, -1),
+        w_gate,
+        w_up,
+        w_down,
+    )
+
+
+def fits_pairs(n_sp, n_tp, operands):
+    queries, w_key, w_gate, w_down = operands[0], operands[3], operands[8], operands[10]
+    return (
+        n_tp == 4
+        and n_sp % n_tp == 0
+        and (n_sp & (n_sp - 1)) == 0
+        and queries.shape[0] % 64 == 0
+        and n_sp * queries.shape[0] <= 1536
+        and (w_key.shape[1] // NOPE) % 2 == 0
+        and w_gate.shape[1] % (2 * LANES) == 0
+        and w_gate.shape[0] % 32 == 0
+        and w_down.shape[1] % LANES == 0
+    )
+
+
 def local(
     queries,
     latents,
@@ -529,6 +1239,10 @@
 ):
     n_sp = lax.axis_size("sp")
     n_tp = lax.axis_size("tp")
+    operands = (queries, latents, rope_key, w_key, w_value, w_out, resid, gain_mix)
+    operands += (w_gate, w_up, w_down, gain_out)
+    if fits_pairs(n_sp, n_tp, operands):
+        return paired_call(n_sp, n_tp, operands)
     rows = queries.shape[0]
     head_count = w_key.shape[1] // NOPE
     rank = latents.shape[1]

time: 123 us -> 110 us (0.89)
  Pallas kernels: 120 us -> 108 us
  local copies, waits for them, and re-layouts: 3.05 us -> 1.62 us
    pallas_call x1, Pallas kernels: 120 us -> 108 us  [paired_call(): pl.pallas_call(functools.partial(paired_kernel, n_sp, n_tp, pieces), out_...]
    unnamed x2 -> x1, local copies, waits for them, and re-layouts: 3.05 us -> 1.62 us
where the time goes in v1:
time: 110 us
  Pallas kernels  108 us (98%)
  local copies, waits for them, and re-layouts  1.62 us (1%)
    pallas_call x1, Pallas kernels, paired_call(): pl.pallas_call(functools.partial(paired_kernel, n_sp, n_tp, pieces), out_...  108 us

profile of v1, /device:TPU:0, one launch (start us, length us, event | category | flops | bytes accessed | tf_op | source)
XLA Modules:
  0.0 109.5 jit_solution(14238919932433703090)
XLA Ops:
  0.0 107.9 %shard_map.118 = bf16[192,512]{1,0:T(8,128)(2,1)} custom-call(bf16[192,384]{1,0:T(8,128)(2,1)} %q_in.1, bf16[4,48,512]{2,1,0:T(8,128)(2,1)} %bitcast.4, bf16[32,192]{1,0:T(8,128)(2,1)} %bitcast.5, bf16[512,256]{1,0:T(8,128)(2,1)} %wk_in.1, bf16[512,256]{1,0:T(8,128)(2,1)} %wv_in.1, bf16[256,2048]{1,0:T(8,128)(2,1)} %wo_ref.1, bf16[192,512]{1,0:T(8,128)(2,1)} %resid_in.1, ...), custom_call_target="tpu_custom_call" | custom-call | tf_op jit(solution)/shard_map/pallas_call | solution.py:1154
  107.9 1.6 %copy.14 = bf16[192,512]{1,0:T(8,128)(2,1)} copy(bf16[192,512]{1,0:T(8,128)(2,1)} %shard_map.118) | data formatting | bytes 393216

commit v2 on v0

--- a/solution.py
+++ b/solution.py
@@ -513,6 +513,717 @@
     return attend(head, at, state)
 
 
+def flip(value, mask):
+    result = value
+    bit = 1
+    while bit <= mask:
+        if mask & bit:
+            result = result + bit - 2 * bit * ((value // bit) % 2)
+        bit *= 2
+    return result
+
+
+class Semaphores:
+    def __init__(self, refs):
+        self.refs, self.base, self.used = refs, {}, 0
+
+    def at(self, name, count=1, index=0):
+        if name not in self.base:
+            self.base[name] = self.used
+            self.used += count
+        return self.refs.at[self.base[name] + index]
+
+
+def paired_kernel(
+    n_sp,
+    n_tp,
+    pieces,
+    q_in,
+    lat_ref,
+    rope_in,
+    wk_in,
+    wv_in,
+    wo_ref,
+    resid_in,
+    gain_mix_in,
+    gain_out_in,
+    wg_ref,
+    wu_ref,
+    wd_ref,
+    out_ref,
+    q_ref,
+    rope_ref,
+    wk_ref,
+    wv_ref,
+    resid_ref,
+    gain_mix_ref,
+    gain_out_ref,
+    lat_all,
+    keys,
+    rotary,
+    values,
+    q_all,
+    heads_all,
+    wo_all,
+    wide_all,
+    down_own,
+    down_all,
+    rows_all,
+    hid,
+    summed,
+    core_send,
+    core_recv,
+    far_send,
+    far_recv,
+    pair_send,
+    pair_recv,
+    stat_send,
+    stat_recv,
+    local_sem,
+    remote_sem,
+):
+    sp = lax.axis_index("sp")
+    tp = lax.axis_index("tp")
+    n_hi = n_sp // 2
+    z, x = sp // 2, sp % 2
+    half = z % 2
+    edge = half == (z // 2) % 2
+    inner = jnp.logical_not(edge)
+    n_rows = q_ref.shape[0]
+    head_count = wk_ref.shape[1] // NOPE
+    rank = wk_ref.shape[0]
+    lat_rows = lat_all.shape[2]
+    n_cols = out_ref.shape[1]
+    group = n_sp // n_tp
+    depth = wg_ref.shape[0]
+    width = wg_ref.shape[1] // 2
+    piece_cols = wd_ref.shape[1] // pieces
+    local_sems = Semaphores(local_sem)
+    remote_sems = Semaphores(remote_sem)
+
+    order = [(1, flip(z, 1))]
+    for m in range(2, n_hi, 2):
+        low, high = flip(z, m), flip(z, m + 1)
+        order.append((jnp.where(edge, m, m + 1), jnp.where(edge, low, high)))
+        order.append((jnp.where(edge, m + 1, m), jnp.where(edge, high, low)))
+    near, rest = list(range(1, len(order), 2)), list(range(2, len(order), 2))
+
+    def sp_of(place, side):
+        return 2 * place + side
+
+    def remote(source, target, device, sent, name, count=1, index=0):
+        return pltpu.make_async_remote_copy(
+            src_ref=source,
+            dst_ref=target,
+            send_sem=remote_sems.at(("sent", sent)),
+            recv_sem=remote_sems.at(name, count, index),
+            device_id=device,
+            device_id_type=MESH,
+        )
+
+    other_x = 1 - x
+    partner, across, corner = flip(tp, 1), flip(tp, 2), flip(tp, 3)
+    to_x = {"sp": sp_of(z, other_x)}
+    to_pair = {"sp": sp_of(flip(z, 1), x)}
+    to_core = {"tp": partner}
+    to_across = {"tp": across}
+
+    barrier = pltpu.get_barrier_semaphore()
+    peers = [{"sp": sp_of(flip(z, k), x)} for k in range(1, n_hi)] + [to_x]
+    peers += [{"tp": flip(tp, j)} for j in range(1, n_tp)]
+    for device in peers:
+        pl.semaphore_signal(barrier, inc=1, device_id=device, device_id_type=MESH)
+
+    def local(source, target, name):
+        return pltpu.make_async_copy(source, target, local_sems.at(name))
+
+    inputs = {
+        "rope": local(rope_in, rope_ref, "rope"),
+        "q": local(q_in, q_ref, "q"),
+        "wk": local(wk_in, wk_ref, "wk"),
+        "wv": local(wv_in, wv_ref, "wv"),
+        "resid": local(resid_in, resid_ref, "resid"),
+        "mix": local(gain_mix_in, gain_mix_ref, "mix"),
+        "out": local(gain_out_in, gain_out_ref, "out"),
+    }
+
+    wide_rows = depth // pieces
+
+    def wide_source(array, which, piece):
+        columns = pl.ds(pl.multiple_of(which * width, LANES), width)
+        return (wg_ref, wu_ref)[array].at[pl.ds(piece * wide_rows, wide_rows), columns]
+
+    def wide_block(array, place, side, piece):
+        rows = pl.ds(piece * wide_rows, wide_rows)
+        return wide_all.at[sp_of(place, side), rows, pl.ds(array * width, width)]
+
+    def down_rows(which, piece):
+        rows = pl.ds(pl.multiple_of(which * width, 16), width)
+        return wd_ref.at[rows, pl.ds(piece * piece_cols, piece_cols)]
+
+    def down_block(place, side, piece):
+        return down_all.at[place * pieces + piece, side]
+
+    def weight_source(array, which, piece):
+        if array == 2:
+            return down_own.at[which, piece]
+        return wide_source(array, which, piece)
+
+    def weight_block(array, place, side, piece):
+        if array == 2:
+            return down_block(place, side, piece)
+        return wide_block(array, place, side, piece)
+
+    def sent_of(array):
+        return "down" if array == 2 else "wide"
+
+    def weight_out(array, k, piece):
+        place = flip(z, k)
+        remote(
+            weight_source(array, place % 2, piece),
+            weight_block(array, z, x, piece),
+            {"sp": sp_of(place, x)},
+            sent_of(array),
+            ("wz", array, piece),
+            n_hi - 1,
+            k - 1,
+        ).start()
+
+    def weight_side(array, k, place, piece, source=None):
+        block = weight_block(array, place, x, piece)
+        name = ("wx", piece) if array == 2 else "wx"
+        count, index = (n_hi, k) if array == 2 else (1, 0)
+        source = block if source is None else source
+        remote(source, block, to_x, sent_of(array), name, count, index).start()
+
+    def weight_own(array, piece):
+        weight_side(array, 0, z, piece, weight_source(array, half, piece))
+
+    def relay(array, at, piece):
+        k, place = order[at]
+        block = weight_block(array, place, x, piece)
+        remote(
+            block, block, to_x, sent_of(array), ("wz", array, piece), n_hi - 1, k - 1
+        ).wait_recv()
+        weight_side(array, k, place, piece)
+
+    def relay_all(array, at):
+        for piece in range(pieces):
+            relay(array, at, piece)
+
+    lat_own = local(lat_ref, lat_all.at[sp, :, :, pl.ds(0, rank)], "lat")
+    inputs["rope"].start()
+    lat_own.start()
+    for name in ("q", "wk", "wv", "resid", "mix", "out"):
+        inputs[name].start()
+    staged = []
+    for piece in range(pieces):
+        for which in range(2):
+            name = ("staged", which, piece)
+            staged.append(local(down_rows(which, piece), down_own.at[which, piece], name))
+            staged[-1].start()
+        for array in range(2):
+            local(
+                weight_source(array, half, piece), weight_block(array, z, x, piece), "wide"
+            ).start()
+    down_mine = []
+    for piece in range(pieces):
+        down_mine.append(
+            local(down_rows(half, piece), down_block(z, x, piece), ("down", piece))
+        )
+        down_mine[-1].start()
+
+    def wo_columns(which):
+        return wo_ref.at[:, pl.ds(pl.multiple_of(which * n_cols, LANES), n_cols)]
+
+    wo_own = local(wo_columns(tp), wo_all.at[tp], "wo")
+    wo_own.start()
+    cosine, sine = rotary_tables(sp * n_rows, n_rows)
+    inputs["rope"].wait()
+    turned_in = jnp.concatenate(
+        [rope_ref[...].astype(jnp.float32), jnp.zeros((LANES - ROPE, n_rows), jnp.float32)],
+        axis=0,
+    )
+    key_rot = rotate(jnp.transpose(turned_in)[:, :ROPE], cosine, sine)
+    key_rot.append(jnp.zeros((n_rows, LANES - ROPE), jnp.float32))
+    lat_all[sp, :, :, pl.ds(rank, LANES)] = (
+        jnp.concatenate(key_rot, axis=1).astype(jnp.bfloat16).reshape(n_tp, lat_rows, LANES)
+    )
+
+    def prepare_queries(head):
+        base = head * (NOPE + ROPE)
+        wide_q = q_ref[...].astype(jnp.float32)
+        nope = wide_q[:, base : base + NOPE]
+        other = jnp.zeros((n_rows, NOPE), jnp.float32)
+        turned = rotate(wide_q[:, base + NOPE : base + NOPE + ROPE], cosine, sine)
+        parts = [nope, other] if head % 2 == 0 else [other, nope]
+        parts = parts + turned + [jnp.zeros((n_rows, LANES - ROPE), jnp.float32)]
+        q_all[head] = jnp.concatenate(parts, axis=1).astype(jnp.bfloat16)
+
+    pl.semaphore_wait(barrier, len(peers))
+    lat_own.wait()
+    for copy in staged:
+        copy.wait()
+
+    def lat_copy(name, k, place, side, quarter, device):
+        block = lat_all.at[sp_of(place, side), quarter]
+        return remote(block, block, device, "lat", ("lat", name), n_hi, k)
+
+    def lat_core(place, side, quarter):
+        block = lat_all.at[sp_of(place, side), quarter]
+        remote(block, block, to_core, "lat", "latc").start()
+
+    def lat_z_in(at):
+        k, place = order[at]
+        lat_copy("z", k, place, x, tp, to_x).wait_recv()
+        lat_copy("x", k, place, x, tp, to_x).start()
+        lat_copy("y", k, place, x, tp, to_across).start()
+        lat_core(place, x, tp)
+
+    def lat_x_in(at):
+        k, place = (0, z) if at is None else order[at]
+        lat_copy("x", k, place, other_x, tp, to_x).wait_recv()
+        if at is not None:
+            lat_copy("yd", k, place, other_x, tp, to_across).start()
+        lat_core(place, other_x, tp)
+
+    def lat_y_in(at):
+        k, place = order[at]
+        lat_copy("y", k, place, x, across, to_across).wait_recv()
+        lat_core(place, x, across)
+
+    def lat_yd_in(at):
+        k, place = order[at]
+        lat_copy("yd", k, place, other_x, across, to_across).wait_recv()
+        lat_core(place, other_x, across)
+
+    for k in range(1, n_hi):
+        block = lat_all.at[sp, tp]
+        remote(
+            block, block, {"sp": sp_of(flip(z, k), x)}, "lat", ("lat", "z"), n_hi, k
+        ).start()
+    lat_copy("x", 0, z, x, tp, to_x).start()
+    block = lat_all.at[sp, across]
+    remote(block, block, to_x, "lat", ("lat", "xa")).start()
+    weight_own(0, 0)
+
+    far = list(range(2, n_hi))
+
+    def send_near(arrays):
+        for array in arrays:
+            for piece in range(pieces):
+                weight_out(array, 1, piece)
+
+    def send_far(array, which):
+        for piece in which:
+            for k in far:
+                weight_out(array, k, piece)
+
+    every = range(pieces)
+    early, late = range(pieces // 2), range(pieces // 2, pieces)
+
+    @pl.when(edge)
+    def outer_first():
+        send_near((0, 1))
+        send_far(0, every)
+        send_far(1, early)
+
+    inputs["q"].wait()
+    prepare_queries(0)
+    lat_x_in(None)
+    lat_z_in(0)
+
+    @pl.when(inner)
+    def inner_first():
+        send_near((0, 1, 2))
+        send_far(0, every)
+        send_far(1, every)
+
+    prepare_queries(1)
+    block = lat_all.at[sp_of(z, other_x), across]
+    remote(block, block, to_x, "lat", ("lat", "xa")).wait_recv()
+    lat_core(z, other_x, across)
+    for at in near:
+        lat_z_in(at)
+    lat_x_in(0)
+    lat_y_in(0)
+    for at in rest:
+        lat_z_in(at)
+    for piece in range(1, pieces):
+        weight_own(0, piece)
+    for piece in range(pieces):
+        weight_own(1, piece)
+    for head in range(2, head_count):
+        prepare_queries(head)
+    for at in near:
+        lat_x_in(at)
+        lat_y_in(at)
+    lat_yd_in(0)
+    for at in rest:
+        lat_x_in(at)
+        lat_y_in(at)
+    for j in (2, 3, 1):
+        to = flip(tp, j)
+        remote(wo_columns(to), wo_all.at[tp], {"tp": to}, "wo", "wo").start()
+    for at in near + rest:
+        lat_yd_in(at)
+    relay_all(0, 0)
+    whole = lat_all.at[pl.ds(0, n_sp - 1), pl.ds(0, 2)]
+    remote(whole, whole, to_core, "lat", "latc").wait_recv()
+
+    half_blocks = n_sp // 2
+
+    def project(step):
+        rows = half_blocks * n_rows
+        blocks = pl.ds(step * half_blocks, half_blocks)
+        lat = lat_all[blocks, :, :, pl.ds(0, rank)].reshape(rows, rank)
+        rotary[pl.ds(step * rows, rows)] = lat_all[blocks, :, :, pl.ds(rank, LANES)].reshape(
+            rows, LANES
+        )
+        keys[pl.ds(step * rows, rows)] = dot(lat, wk_ref[...]).astype(jnp.bfloat16)
+        values[pl.ds(step * rows, rows)] = dot(lat, wv_ref[...]).astype(jnp.bfloat16)
+
+    inputs["wk"].wait()
+    inputs["wv"].wait()
+    for step in range(n_sp // half_blocks):
+        project(step)
+
+    score_scale = (NOPE + ROPE) ** (-0.5)
+    lane = lax.broadcasted_iota(jnp.int32, (n_rows, LANES), 1)
+
+    for head in range(head_count):
+        pair = slice(head // 2 * LANES, (head // 2 + 1) * LANES)
+        whole_keys = jnp.concatenate([keys[:, pair], rotary[...]], axis=1)
+        scores = dot_nt(q_all[head], whole_keys) * score_scale
+        top = jnp.max(scores, axis=1, keepdims=True)
+        probs = jnp.exp(scores - top)
+        sums = jnp.sum(probs, axis=1, keepdims=True)
+        result = dot(probs.astype(jnp.bfloat16), values[:, pair]) / sums
+        if head % 2 == 0:
+            held = result
+        else:
+            heads_all[tp, :, pair] = jnp.where(lane < VDIM, held, result).astype(jnp.bfloat16)
+            block = heads_all.at[tp, :, pl.ds(head // 2 * LANES, LANES)]
+            for j in (2, 3, 1):
+                remote(block, block, {"tp": flip(tp, j)}, "heads", "heads").start()
+        if head == head_count // 2 - 1:
+            relay_all(1, 0)
+        if head == head_count // 2:
+            for at in near:
+                relay_all(0, at)
+
+    for at in rest:
+        relay_all(0, at)
+    for name in ("resid", "mix", "out"):
+        inputs[name].wait()
+    mixed = DEEP_ALPHA * resid_ref[...].astype(jnp.float32)
+    wo_own.wait()
+    mixed = mixed + dot(heads_all[tp], wo_all[tp])
+    others = pl.ds(0, n_tp - 1)
+    remote(wo_all.at[others], wo_all.at[others], to_core, "wo", "wo").wait_recv()
+    remote(heads_all.at[others], heads_all.at[others], to_core, "heads", "heads").wait_recv()
+    for j in (1, 2, 3):
+        sender = flip(tp, j)
+        mixed = mixed + dot(heads_all[sender], wo_all[sender])
+
+    width_total = n_cols * n_tp
+
+    def normed(rows_in, gain_ref, stage, between):
+        sums = jnp.sum(rows_in, axis=1, keepdims=True)
+        squares = jnp.sum(rows_in * rows_in, axis=1, keepdims=True)
+        mine = jnp.transpose(jnp.where(lane < 4, sums, squares))[:8]
+        stat_send[stage] = mine
+        for j in (2, 3, 1):
+            remote(
+                stat_send.at[stage],
+                stat_recv.at[stage, j - 1],
+                {"tp": flip(tp, j)},
+                ("stat", stage),
+                ("stat", stage),
+            ).start()
+        between()
+        arrived = stat_recv.at[stage]
+        remote(arrived, arrived, to_core, ("stat", stage), ("stat", stage)).wait_recv()
+        for j in (1, 2, 3):
+            mine = mine + stat_recv[stage, j - 1]
+        whole = jnp.transpose(mine) / width_total
+        row_mean = whole[:, :1]
+        variance = whole[:, 4:5] - row_mean * row_mean
+        return (
+            (rows_in - row_mean) * lax.rsqrt(variance + NORM_EPSILON) * gain_ref[...]
+        ).astype(jnp.bfloat16)
+
+    def more_down():
+        for piece in range(pieces):
+            weight_own(2, piece)
+
+    hidden_in = normed(mixed, gain_mix_ref, 0, more_down)
+    mine = pl.ds(pl.multiple_of(half * n_rows, 16), n_rows)
+    theirs = pl.ds(pl.multiple_of((1 - half) * n_rows, 16), n_rows)
+    rows_all[tp, mine] = hidden_in
+
+    def rows_copy(name, owner, rows, device):
+        block = rows_all.at[owner, rows]
+        return remote(block, block, device, "rows", ("rows", name))
+
+    def rows_core(owner, rows):
+        block = rows_all.at[owner, rows]
+        remote(block, block, to_core, "rowsc", "rowsc").start()
+
+    rows_copy("y", tp, mine, to_across).start()
+    rows_copy("z", tp, mine, to_pair).start()
+    rows_core(tp, mine)
+
+    @pl.when(edge)
+    def outer_last():
+        send_far(1, late)
+        send_near((2,))
+        send_far(2, every)
+
+    @pl.when(inner)
+    def inner_last():
+        send_far(2, every)
+
+    for at in near:
+        relay_all(1, at)
+    rows_copy("z", tp, theirs, to_pair).wait_recv()
+    rows_copy("yz", tp, theirs, to_across).start()
+    rows_core(tp, theirs)
+    rows_copy("y", across, mine, to_across).wait_recv()
+    rows_core(across, mine)
+    rows_copy("yz", across, theirs, to_across).wait_recv()
+    rows_core(across, theirs)
+    for at in rest:
+        relay_all(1, at)
+    for at in near:
+        relay_all(2, at)
+    both = rows_all.at[pl.ds(0, 2)]
+    remote(both, both, to_core, "rowsc", "rowsc").wait_recv()
+    local(wg_ref, wide_all.at[0], "wide").wait()
+    arrived = wide_all.at[pl.ds(0, n_hi)]
+    remote(arrived, arrived, to_x, "wide", "wx").wait_recv()
+
+    total = None
+    for t in range(n_tp):
+        term = dot(
+            rows_all[t], wide_all[t * group : (t + 1) * group].reshape(group * depth, 2 * width)
+        )
+        total = term if total is None else total + term
+    gate_sum, up_sum = total[:, :width], total[:, width:]
+    hid[...] = (gate_sum / (1.0 + jnp.exp(-gate_sum)) * up_sum).astype(jnp.bfloat16)
+    for copy in down_mine:
+        copy.wait()
+
+    steps = [(None, piece) for piece in range(pieces)] + [(0, piece) for piece in range(pieces)]
+    for first, second in zip(near, rest):
+        steps += [(first, piece) for piece in range(pieces)]
+        steps += [(second, piece) for piece in range(pieces)]
+
+    def facts(at, piece):
+        k, place = (0, z) if at is None else order[at]
+        unit = place * pieces + piece
+        return k, place, unit, tp % 2 == place % 2, tp // 2 == place // 2
+
+    def core_copy(place, unit, piece):
+        return remote(
+            core_send.at[unit],
+            core_recv.at[unit],
+            to_core,
+            "core",
+            "core",
+            n_tp // 2 * pieces,
+            place // 2 * pieces + piece,
+        )
+
+    def far_copy(piece):
+        return remote(
+            far_send.at[piece], far_recv.at[piece], to_across, "far", "far", pieces, piece
+        )
+
+    def pair_copy(piece):
+        return remote(
+            pair_send.at[piece], pair_recv.at[piece], to_pair, "pair", "pair", pieces, piece
+        )
+
+    def make_block(at, piece):
+        k, place, unit, same_core, same_chip = facts(at, piece)
+        block = down_block(place, other_x, piece)
+        remote(block, block, to_x, "down", ("wx", piece), n_hi, k).wait_recv()
+        columns = jnp.concatenate([down_all[unit, 0], down_all[unit, 1]], axis=1)
+        product = dot(hid[...], columns)
+
+        @pl.when(same_core)
+        def keep():
+            summed[unit] = product
+
+        @pl.when(jnp.logical_not(same_core))
+        def give():
+            core_send[unit] = product.astype(jnp.bfloat16)
+            core_copy(place, unit, piece).start()
+
+    def add_core(at, piece):
+        k, place, unit, same_core, same_chip = facts(at, piece)
+
+        @pl.when(same_core)
+        def add():
+            core_copy(place, unit, piece).wait_recv()
+            both = summed[unit] + core_recv[unit].astype(jnp.float32)
+
+            @pl.when(same_chip)
+            def keep():
+                summed[unit] = both
+
+            @pl.when(jnp.logical_not(same_chip))
+            def give():
+                far_send[piece] = both.astype(jnp.bfloat16)
+                far_copy(piece).start()
+
+    def add_far(at, piece):
+        k, place, unit, same_core, same_chip = facts(at, piece)
+
+        @pl.when(place == tp)
+        def add():
+            far_copy(piece).wait_recv()
+            summed[unit, mine] = summed[unit, mine] + far_recv[piece, mine].astype(jnp.float32)
+            pair_send[piece] = (
+                summed[unit, theirs] + far_recv[piece, theirs].astype(jnp.float32)
+            ).astype(jnp.bfloat16)
+            pair_copy(piece).start()
+
+    for at in [0] + rest:
+        relay_all(2, at)
+    ready = [step for step in steps if step[0] not in rest]
+    waiting = [step for step in steps if step[0] in rest]
+    for step in ready:
+        make_block(*step)
+    for step in ready:
+        add_core(*step)
+    for step in waiting:
+        make_block(*step)
+    for step in waiting:
+        add_core(*step)
+    for step in ready + waiting:
+        add_far(*step)
+
+    final = []
+    for piece in range(pieces):
+        pair_copy(piece).wait_recv()
+        final.append(summed[tp * pieces + piece, mine] + pair_recv[piece].astype(jnp.float32))
+    sides = []
+    for side in range(2):
+        for piece in range(pieces):
+            sides.append(final[piece][:, side * piece_cols : (side + 1) * piece_cols])
+    mixer = jnp.concatenate(sides, axis=1)
+    last_in = DEEP_ALPHA * rows_all[tp, mine].astype(jnp.float32) + HALF_STEP * mixer
+    out_ref[...] = normed(last_in, gain_out_ref, 1, lambda: None)
+
+    def all_sent(sent, name, whole):
+        remote(whole, whole, to_core, sent, name).wait_send()
+
+    all_sent("lat", "latc", lat_all.at[pl.ds(0, n_sp - 1)])
+    all_sent("wide", "wx", wide_all.at[pl.ds(0, n_sp - 1)])
+    all_sent("down", "wx", down_all.at[pl.ds(0, (n_sp - 1) * pieces // 2)])
+    all_sent("wo", "wo", wo_all.at[others])
+    all_sent("heads", "heads", heads_all.at[others])
+    all_sent("rows", ("rows", "z"), rows_all.at[others, pl.ds(0, n_rows)])
+    all_sent("rowsc", "rowsc", both)
+    for stage in range(2):
+        all_sent(("stat", stage), ("stat", stage), stat_recv.at[stage])
+    all_sent("core", "core", core_send.at[pl.ds(0, n_hi * pieces // 2)])
+    all_sent("far", "far", far_send)
+    all_sent("pair", "pair", pair_send)
+
+
+def paired_call(n_sp, n_tp, operands):
+    queries, latents, rope_key, w_key, w_value, w_out, resid, gain_mix = operands[:8]
+    w_gate, w_up, w_down, gain_out = operands[8:]
+    rows = queries.shape[0]
+    head_count = w_key.shape[1] // NOPE
+    rank = latents.shape[1]
+    cols = resid.shape[1]
+    depth, hidden_width = w_gate.shape
+    width = hidden_width // 2
+    pieces = 2
+    n_hi = n_sp // 2
+    unit_cols = 2 * w_down.shape[1] // pieces
+    total_rows = n_sp * rows
+    bf16 = jnp.bfloat16
+    f32 = jnp.float32
+    vmem = pl.BlockSpec(memory_space=pltpu.VMEM)
+    anywhere = pl.BlockSpec(memory_space=pl.ANY)
+    dma = pltpu.SemaphoreType.DMA
+    signals = 18 + 5 * n_hi + 2 * (n_hi - 1) * pieces + (2 * n_hi - 1) * pieces + 11
+    signals += (n_tp // 2 + 2) * pieces + 4
+    return pl.pallas_call(
+        functools.partial(paired_kernel, n_sp, n_tp, pieces),
+        out_shape=jax.ShapeDtypeStruct((rows, cols), bf16),
+        in_specs=[anywhere] * 12,
+        out_specs=vmem,
+        scratch_shapes=[
+            pltpu.VMEM(queries.shape, bf16),
+            pltpu.VMEM((rope_key.shape[1], rows), bf16),
+            pltpu.VMEM(w_key.shape, bf16),
+            pltpu.VMEM(w_value.shape, bf16),
+            pltpu.VMEM(resid.shape, bf16),
+            pltpu.VMEM((1, cols), f32),
+            pltpu.VMEM((1, cols), f32),
+            pltpu.VMEM((n_sp, n_tp, rows // n_tp, rank + LANES), bf16),
+            pltpu.VMEM((total_rows, head_count * NOPE), bf16),
+            pltpu.VMEM((total_rows, LANES), bf16),
+            pltpu.VMEM((total_rows, head_count * VDIM), bf16),
+            pltpu.VMEM((head_count, rows, 2 * LANES), bf16),
+            pltpu.VMEM((n_tp, rows, head_count * VDIM), bf16),
+            pltpu.VMEM((n_tp, head_count * VDIM, cols), bf16),
+            pltpu.VMEM((n_sp, depth, 2 * width), bf16),
+            pltpu.VMEM((2, pieces, width, unit_cols // 2), bf16),
+            pltpu.VMEM((n_hi * pieces, 2, width, unit_cols // 2), bf16),
+            pltpu.VMEM((n_tp, 2 * rows, cols), bf16),
+            pltpu.VMEM((2 * rows, width), bf16),
+            pltpu.VMEM((n_hi * pieces, 2 * rows, unit_cols), f32),
+            pltpu.VMEM((n_hi * pieces, 2 * rows, unit_cols), bf16),
+            pltpu.VMEM((n_hi * pieces, 2 * rows, unit_cols), bf16),
+            pltpu.VMEM((pieces, 2 * rows, unit_cols), bf16),
+            pltpu.VMEM((pieces, 2 * rows, unit_cols), bf16),
+            pltpu.VMEM((pieces, rows, unit_cols), bf16),
+            pltpu.VMEM((pieces, rows, unit_cols), bf16),
+            pltpu.VMEM((2, 8, rows), f32),
+            pltpu.VMEM((2, n_tp - 1, 8, rows), f32),
+            dma((10 + 3 * pieces,)),
+            dma((signals,)),
+        ],
+        compiler_params=pltpu.CompilerParams(
+            collective_id=1, has_side_effects=True, vmem_limit_bytes=66000000
+        ),
+    )(
+        queries,
+        latents.reshape(n_tp, rows // n_tp, rank),
+        rope_key.T,
+        w_key,
+        w_value,
+        w_out,
+        resid,
+        gain_mix.reshape(1, -1),
+        gain_out.reshape(1, -1),
+        w_gate,
+        w_up,
+        w_down,
+    )
+
+
+def fits_pairs(n_sp, n_tp, operands):
+    queries, w_key, w_gate, w_down = operands[0], operands[3], operands[8], operands[10]
+    return (
+        n_tp == 4
+        and n_sp == 2 * n_tp
+        and queries.shape[0] % 64 == 0
+        and n_sp * queries.shape[0] <= 1536
+        and (w_key.shape[1] // NOPE) % 2 == 0
+        and w_gate.shape[1] % (2 * LANES) == 0
+        and w_gate.shape[0] % 32 == 0
+        and w_down.shape[1] % (2 * LANES) == 0
+    )
+
+
 def local(
     queries,
     latents,
@@ -529,6 +1240,10 @@
 ):
     n_sp = lax.axis_size("sp")
     n_tp = lax.axis_size("tp")
+    operands = (queries, latents, rope_key, w_key, w_value, w_out, resid, gain_mix)
+    operands += (w_gate, w_up, w_down, gain_out)
+    if fits_pairs(n_sp, n_tp, operands):
+        return paired_call(n_sp, n_tp, operands)
     rows = queries.shape[0]
     head_count = w_key.shape[1] // NOPE
     rank = latents.shape[1]

time: 123 us -> 94 us (0.76)
  Pallas kernels: 120 us -> 92.1 us
  local copies, waits for them, and re-layouts: 3.05 us -> 1.62 us
    pallas_call x1, Pallas kernels: 120 us -> 92.1 us  [paired_call(): pl.pallas_call(functools.partial(paired_kernel, n_sp, n_tp, pieces), out_...]
    unnamed x2 -> x1, local copies, waits for them, and re-layouts: 3.05 us -> 1.62 us
where the time goes in v2:
time: 94 us; the launch traced here: 93.8 us
  Pallas kernels  92.1 us (98%)
  local copies, waits for them, and re-layouts  1.62 us (2%)
    pallas_call x1, Pallas kernels, paired_call(): pl.pallas_call(functools.partial(paired_kernel, n_sp, n_tp, pieces), out_...  92.1 us

profile of v2, /device:TPU:0, one launch (start us, length us, event | category | flops | bytes accessed | tf_op | source)
XLA Modules:
  0.0 93.8 jit_solution(17400450348143596592)
XLA Ops:
  0.0 92.1 %shard_map.118 = bf16[192,512]{1,0:T(8,128)(2,1)} custom-call(bf16[192,384]{1,0:T(8,128)(2,1)} %q_in.1, bf16[4,48,512]{2,1,0:T(8,128)(2,1)} %bitcast.4, bf16[32,192]{1,0:T(8,128)(2,1)} %bitcast.5, bf16[512,256]{1,0:T(8,128)(2,1)} %wk_in.1, bf16[512,256]{1,0:T(8,128)(2,1)} %wv_in.1, bf16[256,2048]{1,0:T(8,128)(2,1)} %wo_ref.1, bf16[192,512]{1,0:T(8,128)(2,1)} %resid_in.1, ...), custom_call_target="tpu_custom_call" | custom-call | tf_op jit(solution)/shard_map/pallas_call | solution.py:1157
  92.1 1.6 %copy.14 = bf16[192,512]{1,0:T(8,128)(2,1)} copy(bf16[192,512]{1,0:T(8,128)(2,1)} %shard_map.118) | data formatting | bytes 393216

commit v3 on v2

--- a/solution.py
+++ b/solution.py
@@ -577,6 +577,11 @@
     far_recv,
     pair_send,
     pair_recv,
+    first_send,
+    first_recv,
+    last_send,
+    last_recv,
+    total_sum,
     stat_send,
     stat_recv,
     local_sem,
@@ -828,16 +833,16 @@
         send_far(0, every)
         send_far(1, early)
 
-    inputs["q"].wait()
-    prepare_queries(0)
-    lat_x_in(None)
-    lat_z_in(0)
-
     @pl.when(inner)
     def inner_first():
         send_near((0, 1, 2))
         send_far(0, every)
         send_far(1, every)
+
+    inputs["q"].wait()
+    prepare_queries(0)
+    lat_x_in(None)
+    lat_z_in(0)
 
     prepare_queries(1)
     block = lat_all.at[sp_of(z, other_x), across]
@@ -853,6 +858,8 @@
         weight_own(0, piece)
     for piece in range(pieces):
         weight_own(1, piece)
+    for piece in range(pieces):
+        weight_own(2, piece)
     for head in range(2, head_count):
         prepare_queries(head)
     for at in near:
@@ -908,12 +915,6 @@
                 remote(block, block, {"tp": flip(tp, j)}, "heads", "heads").start()
         if head == head_count // 2 - 1:
             relay_all(1, 0)
-        if head == head_count // 2:
-            for at in near:
-                relay_all(0, at)
-
-    for at in rest:
-        relay_all(0, at)
     for name in ("resid", "mix", "out"):
         inputs[name].wait()
     mixed = DEEP_ALPHA * resid_ref[...].astype(jnp.float32)
@@ -953,11 +954,11 @@
             (rows_in - row_mean) * lax.rsqrt(variance + NORM_EPSILON) * gain_ref[...]
         ).astype(jnp.bfloat16)
 
-    def more_down():
-        for piece in range(pieces):
-            weight_own(2, piece)
-
-    hidden_in = normed(mixed, gain_mix_ref, 0, more_down)
+    def more_wide():
+        for at in near + rest:
+            relay_all(0, at)
+
+    hidden_in = normed(mixed, gain_mix_ref, 0, more_wide)
     mine = pl.ds(pl.multiple_of(half * n_rows, 16), n_rows)
     theirs = pl.ds(pl.multiple_of((1 - half) * n_rows, 16), n_rows)
     rows_all[tp, mine] = hidden_in
@@ -986,17 +987,23 @@
 
     for at in near:
         relay_all(1, at)
+    for at in rest:
+        for piece in early:
+            relay(1, at, piece)
     rows_copy("z", tp, theirs, to_pair).wait_recv()
     rows_copy("yz", tp, theirs, to_across).start()
     rows_core(tp, theirs)
     rows_copy("y", across, mine, to_across).wait_recv()
     rows_core(across, mine)
+    for at in rest:
+        for piece in late:
+            relay(1, at, piece)
     rows_copy("yz", across, theirs, to_across).wait_recv()
     rows_core(across, theirs)
-    for at in rest:
-        relay_all(1, at)
+    relay_all(2, 0)
     for at in near:
-        relay_all(2, at)
+        for piece in early:
+            relay(2, at, piece)
     both = rows_all.at[pl.ds(0, 2)]
     remote(both, both, to_core, "rowsc", "rowsc").wait_recv()
     local(wg_ref, wide_all.at[0], "wide").wait()
@@ -1014,11 +1021,6 @@
     for copy in down_mine:
         copy.wait()
 
-    steps = [(None, piece) for piece in range(pieces)] + [(0, piece) for piece in range(pieces)]
-    for first, second in zip(near, rest):
-        steps += [(first, piece) for piece in range(pieces)]
-        steps += [(second, piece) for piece in range(pieces)]
-
     def facts(at, piece):
         k, place = (0, z) if at is None else order[at]
         unit = place * pieces + piece
@@ -1045,6 +1047,14 @@
             pair_send.at[piece], pair_recv.at[piece], to_pair, "pair", "pair", pieces, piece
         )
 
+    def pair_first_copy(piece):
+        source, target = first_send.at[piece], first_recv.at[piece]
+        return remote(source, target, to_pair, "first", "first", pieces, piece)
+
+    def far_last_copy(piece):
+        source, target = last_send.at[piece], last_recv.at[piece]
+        return remote(source, target, to_across, "last", "last", pieces, piece)
+
     def make_block(at, piece):
         k, place, unit, same_core, same_chip = facts(at, piece)
         block = down_block(place, other_x, piece)
@@ -1090,25 +1100,74 @@
             ).astype(jnp.bfloat16)
             pair_copy(piece).start()
 
-    for at in [0] + rest:
-        relay_all(2, at)
-    ready = [step for step in steps if step[0] not in rest]
-    waiting = [step for step in steps if step[0] in rest]
-    for step in ready:
-        make_block(*step)
-    for step in ready:
-        add_core(*step)
-    for step in waiting:
-        make_block(*step)
-    for step in waiting:
-        add_core(*step)
-    for step in ready + waiting:
-        add_far(*step)
-
-    final = []
-    for piece in range(pieces):
-        pair_copy(piece).wait_recv()
-        final.append(summed[tp * pieces + piece, mine] + pair_recv[piece].astype(jnp.float32))
+    def pair_first(at, piece):
+        k, place, unit, same_core, same_chip = facts(at, piece)
+
+        @pl.when(same_core)
+        def add():
+            core_copy(place, unit, piece).wait_recv()
+            first_send[piece] = (
+                summed[unit, theirs] + core_recv[unit, theirs].astype(jnp.float32)
+            ).astype(jnp.bfloat16)
+            pair_first_copy(piece).start()
+
+    def pair_added(at, piece):
+        k, place, unit, same_core, same_chip = facts(at, piece)
+
+        @pl.when(same_core)
+        def add():
+            pair_first_copy(piece).wait_recv()
+            both = summed[unit, mine] + core_recv[unit, mine].astype(jnp.float32)
+            both = both + first_recv[piece].astype(jnp.float32)
+
+            @pl.when(same_chip)
+            def keep():
+                total_sum[piece] = both
+
+            @pl.when(jnp.logical_not(same_chip))
+            def give():
+                last_send[piece] = both.astype(jnp.bfloat16)
+                far_last_copy(piece).start()
+
+    def finish_far(at, piece):
+        k, place, unit, same_core, same_chip = facts(at, piece)
+
+        @pl.when(place == tp)
+        def add():
+            far_last_copy(piece).wait_recv()
+            total_sum[piece] = total_sum[piece] + last_recv[piece].astype(jnp.float32)
+
+    def finish_pair(at, piece):
+        k, place, unit, same_core, same_chip = facts(at, piece)
+
+        @pl.when(place == tp)
+        def add():
+            pair_copy(piece).wait_recv()
+            total_sum[piece] = summed[unit, mine] + pair_recv[piece].astype(jnp.float32)
+
+    def each(apply, ats, which):
+        for piece in which:
+            for at in ats:
+                apply(at, piece)
+
+    close = [None, 0]
+    each(make_block, close, every)
+    each(functools.partial(relay, 2), rest, early)
+    each(add_core, close, every)
+    each(make_block, near, early)
+    each(functools.partial(relay, 2), rest, late)
+    each(make_block, rest, early)
+    each(functools.partial(relay, 2), near, late)
+    each(pair_first, near + rest, early)
+    each(make_block, rest, late)
+    each(make_block, near, late)
+    each(pair_first, rest + near, late)
+    each(add_far, close, every)
+    each(pair_added, near + rest, early)
+    each(pair_added, rest + near, late)
+    each(finish_pair, close, every)
+    each(finish_far, near + rest, every)
+    final = [total_sum[piece] for piece in range(pieces)]
     sides = []
     for side in range(2):
         for piece in range(pieces):
@@ -1130,8 +1189,17 @@
     for stage in range(2):
         all_sent(("stat", stage), ("stat", stage), stat_recv.at[stage])
     all_sent("core", "core", core_send.at[pl.ds(0, n_hi * pieces // 2)])
-    all_sent("far", "far", far_send)
-    all_sent("pair", "pair", pair_send)
+    all_sent("first", "first", first_send)
+    home = tp // 2 == z // 2
+
+    @pl.when(home)
+    def sent_home():
+        all_sent("pair", "pair", pair_send)
+        all_sent("last", "last", last_send)
+
+    @pl.when(jnp.logical_not(home))
+    def sent_away():
+        all_sent("far", "far", far_send)
 
 
 def paired_call(n_sp, n_tp, operands):
@@ -1153,7 +1221,7 @@
     anywhere = pl.BlockSpec(memory_space=pl.ANY)
     dma = pltpu.SemaphoreType.DMA
     signals = 18 + 5 * n_hi + 2 * (n_hi - 1) * pieces + (2 * n_hi - 1) * pieces + 11
-    signals += (n_tp // 2 + 2) * pieces + 4
+    signals += (n_tp // 2 + 4) * pieces + 6
     return pl.pallas_call(
         functools.partial(paired_kernel, n_sp, n_tp, pieces),
         out_shape=jax.ShapeDtypeStruct((rows, cols), bf16),
@@ -1186,6 +1254,11 @@
             pltpu.VMEM((pieces, 2 * rows, unit_cols), bf16),
             pltpu.VMEM((pieces, rows, unit_cols), bf16),
             pltpu.VMEM((pieces, rows, unit_cols), bf16),
+            pltpu.VMEM((pieces, rows, unit_cols), bf16),
+            pltpu.VMEM((pieces, rows, unit_cols), bf16),
+            pltpu.VMEM((pieces, rows, unit_cols), bf16),
+            pltpu.VMEM((pieces, rows, unit_cols), bf16),
+            pltpu.VMEM((pieces, rows, unit_cols), f32),
             pltpu.VMEM((2, 8, rows), f32),
             pltpu.VMEM((2, n_tp - 1, 8, rows), f32),
             dma((10 + 3 * pieces,)),

time: 94 us -> 82.9 us (0.88)
  Pallas kernels: 92.1 us -> 81.1 us
    pallas_call x1, Pallas kernels: 92.1 us -> 81.1 us  [paired_call(): pl.pallas_call(functools.partial(paired_kernel, n_sp, n_tp, pieces), out_...]
where the time goes in v3:
time: 82.9 us; the launch traced here: 82.7 us
  Pallas kernels  81.1 us (98%)
  local copies, waits for them, and re-layouts  1.62 us (2%)
    pallas_call x1, Pallas kernels, paired_call(): pl.pallas_call(functools.partial(paired_kernel, n_sp, n_tp, pieces), out_...  81.1 us

profile of v3, /device:TPU:0, one launch (start us, length us, event | category | flops | bytes accessed | tf_op | source)
XLA Modules:
  0.0 82.7 jit_solution(15747030386641400629)
XLA Ops:
  0.0 81.1 %shard_map.118 = bf16[192,512]{1,0:T(8,128)(2,1)} custom-call(bf16[192,384]{1,0:T(8,128)(2,1)} %q_in.1, bf16[4,48,512]{2,1,0:T(8,128)(2,1)} %bitcast.4, bf16[32,192]{1,0:T(8,128)(2,1)} %bitcast.5, bf16[512,256]{1,0:T(8,128)(2,1)} %wk_in.1, bf16[512,256]{1,0:T(8,128)(2,1)} %wv_in.1, bf16[256,2048]{1,0:T(8,128)(2,1)} %wo_ref.1, bf16[192,512]{1,0:T(8,128)(2,1)} %resid_in.1, ...), custom_call_target="tpu_custom_call" | custom-call | tf_op jit(solution)/shard_map/pallas_call | solution.py:1225
  81.1 1.6 %copy.14 = bf16[192,512]{1,0:T(8,128)(2,1)} copy(bf16[192,512]{1,0:T(8,128)(2,1)} %shard_map.118) | data formatting | bytes 393216

commit v4 on v3

--- a/solution.py
+++ b/solution.py
@@ -682,17 +682,25 @@
     def sent_of(array):
         return "down" if array == 2 else "wide"
 
+    def parts_of(array, ref):
+        if array < 2:
+            return [ref]
+        return [ref.at[pl.ds(part * width // 2, width // 2)] for part in range(2)]
+
     def weight_out(array, k, piece):
         place = flip(z, k)
-        remote(
-            weight_source(array, place % 2, piece),
-            weight_block(array, z, x, piece),
-            {"sp": sp_of(place, x)},
-            sent_of(array),
-            ("wz", array, piece),
-            n_hi - 1,
-            k - 1,
-        ).start()
+        sources = parts_of(array, weight_source(array, place % 2, piece))
+        targets = parts_of(array, weight_block(array, z, x, piece))
+        for part, (source, target) in enumerate(zip(sources, targets)):
+            remote(
+                source,
+                target,
+                {"sp": sp_of(place, x)},
+                sent_of(array),
+                ("wz", array, piece, part),
+                n_hi - 1,
+                k - 1,
+            ).start()
 
     def weight_side(array, k, place, piece, source=None):
         block = weight_block(array, place, x, piece)
@@ -706,11 +714,19 @@
 
     def relay(array, at, piece):
         k, place = order[at]
-        block = weight_block(array, place, x, piece)
-        remote(
-            block, block, to_x, sent_of(array), ("wz", array, piece), n_hi - 1, k - 1
-        ).wait_recv()
-        weight_side(array, k, place, piece)
+        name = ("wx", piece) if array == 2 else "wx"
+        count, index = (n_hi, k) if array == 2 else (1, 0)
+        for part, block in enumerate(parts_of(array, weight_block(array, place, x, piece))):
+            remote(
+                block,
+                block,
+                to_x,
+                sent_of(array),
+                ("wz", array, piece, part),
+                n_hi - 1,
+                k - 1,
+            ).wait_recv()
+            remote(block, block, to_x, sent_of(array), name, count, index).start()
 
     def relay_all(array, at):
         for piece in range(pieces):
@@ -788,8 +804,7 @@
     def lat_x_in(at):
         k, place = (0, z) if at is None else order[at]
         lat_copy("x", k, place, other_x, tp, to_x).wait_recv()
-        if at is not None:
-            lat_copy("yd", k, place, other_x, tp, to_across).start()
+        lat_copy("yd", k, place, other_x, tp, to_across).start()
         lat_core(place, other_x, tp)
 
     def lat_y_in(at):
@@ -798,7 +813,7 @@
         lat_core(place, x, across)
 
     def lat_yd_in(at):
-        k, place = order[at]
+        k, place = (0, z) if at is None else order[at]
         lat_copy("yd", k, place, other_x, across, to_across).wait_recv()
         lat_core(place, other_x, across)
 
@@ -808,8 +823,6 @@
             block, block, {"sp": sp_of(flip(z, k), x)}, "lat", ("lat", "z"), n_hi, k
         ).start()
     lat_copy("x", 0, z, x, tp, to_x).start()
-    block = lat_all.at[sp, across]
-    remote(block, block, to_x, "lat", ("lat", "xa")).start()
     weight_own(0, 0)
 
     far = list(range(2, n_hi))
@@ -845,17 +858,15 @@
     lat_z_in(0)
 
     prepare_queries(1)
-    block = lat_all.at[sp_of(z, other_x), across]
-    remote(block, block, to_x, "lat", ("lat", "xa")).wait_recv()
-    lat_core(z, other_x, across)
+    for piece in range(1, pieces):
+        weight_own(0, piece)
     for at in near:
         lat_z_in(at)
+    lat_yd_in(None)
     lat_x_in(0)
     lat_y_in(0)
     for at in rest:
         lat_z_in(at)
-    for piece in range(1, pieces):
-        weight_own(0, piece)
     for piece in range(pieces):
         weight_own(1, piece)
     for piece in range(pieces):
@@ -915,6 +926,8 @@
                 remote(block, block, {"tp": flip(tp, j)}, "heads", "heads").start()
         if head == head_count // 2 - 1:
             relay_all(1, 0)
+    for at in near:
+        relay_all(0, at)
     for name in ("resid", "mix", "out"):
         inputs[name].wait()
     mixed = DEEP_ALPHA * resid_ref[...].astype(jnp.float32)
@@ -955,7 +968,7 @@
         ).astype(jnp.bfloat16)
 
     def more_wide():
-        for at in near + rest:
+        for at in rest:
             relay_all(0, at)
 
     hidden_in = normed(mixed, gain_mix_ref, 0, more_wide)
@@ -1220,11 +1233,11 @@
     vmem = pl.BlockSpec(memory_space=pltpu.VMEM)
     anywhere = pl.BlockSpec(memory_space=pl.ANY)
     dma = pltpu.SemaphoreType.DMA
-    signals = 18 + 5 * n_hi + 2 * (n_hi - 1) * pieces + (2 * n_hi - 1) * pieces + 11
-    signals += (n_tp // 2 + 4) * pieces + 6
+    signals = 4 * n_hi + 4 * (n_hi - 1) * pieces + n_hi * pieces
+    signals += (n_tp // 2 + 4) * pieces + 24
     return pl.pallas_call(
         functools.partial(paired_kernel, n_sp, n_tp, pieces),
-        out_shape=jax.ShapeDtypeStruct((rows, cols), bf16),
+        out_shape=pltpu.VMEM((rows, cols), bf16),
         in_specs=[anywhere] * 12,
         out_specs=vmem,
         scratch_shapes=[

time: 82.9 us -> 79.7 us (0.961)
  Pallas kernels: 81.1 us -> 78.6 us
  local copies, waits for them, and re-layouts: 1.62 us -> 0.68 us
    pallas_call x1, Pallas kernels: 81.1 us -> 78.6 us  [paired_call(): pl.pallas_call(functools.partial(paired_kernel, n_sp, n_tp, pieces), out_...]
    unnamed x1, local copies, waits for them, and re-layouts: 1.62 us -> 0.68 us
where the time goes in v4:
time: 79.7 us; the launch traced here: 79.3 us
  Pallas kernels  78.6 us (99%)
    pallas_call x1, Pallas kernels, paired_call(): pl.pallas_call(functools.partial(paired_kernel, n_sp, n_tp, pieces), out_...  78.6 us

profile of v4, /device:TPU:0, one launch (start us, length us, event | category | flops | bytes accessed | tf_op | source)
XLA Modules:
  0.0 79.3 jit_solution(1859835447604244046)
XLA Ops:
  0.0 78.6 %shard_map.118 = bf16[192,512]{1,0:T(8,128)(2,1)S(1)} custom-call(bf16[192,384]{1,0:T(8,128)(2,1)} %q_in.1, bf16[4,48,512]{2,1,0:T(8,128)(2,1)} %bitcast.4, bf16[32,192]{1,0:T(8,128)(2,1)} %bitcast.5, bf16[512,256]{1,0:T(8,128)(2,1)} %wk_in.1, bf16[512,256]{1,0:T(8,128)(2,1)} %wv_in.1, bf16[256,2048]{1,0:T(8,128)(2,1)} %wo_ref.1, bf16[192,512]{1,0:T(8,128)(2,1)} %resid_in.1, ...), custom_call_target="tpu_custom_call" | custom-call | tf_op jit(solution)/shard_map/pallas_call | solution.py:1238
  78.6 0.7 copy.14

commit v5 on v4

--- a/solution.py
+++ b/solution.py
@@ -1011,12 +1011,27 @@
     for at in rest:
         for piece in late:
             relay(1, at, piece)
+
+    @pl.when(edge)
+    def outer_first_down():
+        relay_all(2, 0)
+        for at in near:
+            for piece in early:
+                relay(2, at, piece)
+
     rows_copy("yz", across, theirs, to_across).wait_recv()
     rows_core(across, theirs)
-    relay_all(2, 0)
-    for at in near:
-        for piece in early:
-            relay(2, at, piece)
+
+    @pl.when(inner)
+    def inner_first_down():
+        relay_all(2, 0)
+
+    @pl.when(inner)
+    def inner_near_down():
+        for at in near:
+            for piece in early:
+                relay(2, at, piece)
+
     both = rows_all.at[pl.ds(0, 2)]
     remote(both, both, to_core, "rowsc", "rowsc").wait_recv()
     local(wg_ref, wide_all.at[0], "wide").wait()
@@ -1062,11 +1077,11 @@
 
     def pair_first_copy(piece):
         source, target = first_send.at[piece], first_recv.at[piece]
-        return remote(source, target, to_pair, "first", "first", pieces, piece)
+        return remote(source, target, to_pair, "first", "first", pieces + 1, piece)
 
     def far_last_copy(piece):
         source, target = last_send.at[piece], last_recv.at[piece]
-        return remote(source, target, to_across, "last", "last", pieces, piece)
+        return remote(source, target, to_across, "last", "last", pieces + 1, piece)
 
     def make_block(at, piece):
         k, place, unit, same_core, same_chip = facts(at, piece)
@@ -1113,42 +1128,48 @@
             ).astype(jnp.bfloat16)
             pair_copy(piece).start()
 
+    def slot_of(at, piece):
+        return pieces if at is None or at == 0 else piece
+
     def pair_first(at, piece):
         k, place, unit, same_core, same_chip = facts(at, piece)
+        slot = slot_of(at, piece)
 
         @pl.when(same_core)
         def add():
             core_copy(place, unit, piece).wait_recv()
-            first_send[piece] = (
+            first_send[slot] = (
                 summed[unit, theirs] + core_recv[unit, theirs].astype(jnp.float32)
             ).astype(jnp.bfloat16)
-            pair_first_copy(piece).start()
+            pair_first_copy(slot).start()
 
     def pair_added(at, piece):
         k, place, unit, same_core, same_chip = facts(at, piece)
+        slot = slot_of(at, piece)
 
         @pl.when(same_core)
         def add():
-            pair_first_copy(piece).wait_recv()
+            pair_first_copy(slot).wait_recv()
             both = summed[unit, mine] + core_recv[unit, mine].astype(jnp.float32)
-            both = both + first_recv[piece].astype(jnp.float32)
+            both = both + first_recv[slot].astype(jnp.float32)
 
             @pl.when(same_chip)
             def keep():
-                total_sum[piece] = both
+                total_sum[slot] = both
 
             @pl.when(jnp.logical_not(same_chip))
             def give():
-                last_send[piece] = both.astype(jnp.bfloat16)
-                far_last_copy(piece).start()
+                last_send[slot] = both.astype(jnp.bfloat16)
+                far_last_copy(slot).start()
 
     def finish_far(at, piece):
         k, place, unit, same_core, same_chip = facts(at, piece)
+        slot = slot_of(at, piece)
 
         @pl.when(place == tp)
         def add():
-            far_last_copy(piece).wait_recv()
-            total_sum[piece] = total_sum[piece] + last_recv[piece].astype(jnp.float32)
+            far_last_copy(slot).wait_recv()
+            total_sum[piece] = total_sum[slot] + last_recv[slot].astype(jnp.float32)
 
     def finish_pair(at, piece):
         k, place, unit, same_core, same_chip = facts(at, piece)
@@ -1166,19 +1187,22 @@
     close = [None, 0]
     each(make_block, close, every)
     each(functools.partial(relay, 2), rest, early)
-    each(add_core, close, every)
+    each(add_core, close, early)
+    each(pair_first, close, late)
     each(make_block, near, early)
     each(functools.partial(relay, 2), rest, late)
     each(make_block, rest, early)
     each(functools.partial(relay, 2), near, late)
     each(pair_first, near + rest, early)
     each(make_block, rest, late)
+    each(pair_added, close, late)
     each(make_block, near, late)
     each(pair_first, rest + near, late)
-    each(add_far, close, every)
+    each(add_far, close, early)
     each(pair_added, near + rest, early)
     each(pair_added, rest + near, late)
-    each(finish_pair, close, every)
+    each(finish_far, close, late)
+    each(finish_pair, close, early)
     each(finish_far, near + rest, every)
     final = [total_sum[piece] for piece in range(pieces)]
     sides = []
@@ -1204,15 +1228,17 @@
     all_sent("core", "core", core_send.at[pl.ds(0, n_hi * pieces // 2)])
     all_sent("first", "first", first_send)
     home = tp // 2 == z // 2
+    early_rows = pl.ds(0, pieces // 2)
 
     @pl.when(home)
     def sent_home():
-        all_sent("pair", "pair", pair_send)
-        all_sent("last", "last", last_send)
+        all_sent("pair", "pair", pair_send.at[early_rows])
+        all_sent("last", "last", last_send.at[pl.ds(0, pieces)])
 
     @pl.when(jnp.logical_not(home))
     def sent_away():
-        all_sent("far", "far", far_send)
+        all_sent("far", "far", far_send.at[early_rows])
+        all_sent("last", "last", last_send.at[early_rows])
 
 
 def paired_call(n_sp, n_tp, operands):
@@ -1234,7 +1260,7 @@
     anywhere = pl.BlockSpec(memory_space=pl.ANY)
     dma = pltpu.SemaphoreType.DMA
     signals = 4 * n_hi + 4 * (n_hi - 1) * pieces + n_hi * pieces
-    signals += (n_tp // 2 + 4) * pieces + 24
+    signals += (n_tp // 2 + 4) * pieces + 26
     return pl.pallas_call(
         functools.partial(paired_kernel, n_sp, n_tp, pieces),
         out_shape=pltpu.VMEM((rows, cols), bf16),
@@ -1267,11 +1293,11 @@
             pltpu.VMEM((pieces, 2 * rows, unit_cols), bf16),
             pltpu.VMEM((pieces, rows, unit_cols), bf16),
             pltpu.VMEM((pieces, rows, unit_cols), bf16),
-            pltpu.VMEM((pieces, rows, unit_cols), bf16),
-            pltpu.VMEM((pieces, rows, unit_cols), bf16),
-            pltpu.VMEM((pieces, rows, unit_cols), bf16),
-            pltpu.VMEM((pieces, rows, unit_cols), bf16),
-            pltpu.VMEM((pieces, rows, unit_cols), f32),
+            pltpu.VMEM((pieces + 1, rows, unit_cols), bf16),
+            pltpu.VMEM((pieces + 1, rows, unit_cols), bf16),
+            pltpu.VMEM((pieces + 1, rows, unit_cols), bf16),
+            pltpu.VMEM((pieces + 1, rows, unit_cols), bf16),
+            pltpu.VMEM((pieces + 1, rows, unit_cols), f32),
             pltpu.VMEM((2, 8, rows), f32),
             pltpu.VMEM((2, n_tp - 1, 8, rows), f32),
             dma((10 + 3 * pieces,)),

time: 79.7 us -> 79.1 us (level)
  no operation moved by 1% of the time
where the time goes in v5:
time: 79.1 us; the launch traced here: 78.9 us
  Pallas kernels  78.2 us (99%)
    pallas_call x1, Pallas kernels, paired_call(): pl.pallas_call(functools.partial(paired_kernel, n_sp, n_tp, pieces), out_...  78.2 us

profile of v5, /device:TPU:0, one launch (start us, length us, event | category | flops | bytes accessed | tf_op | source)
XLA Modules:
  0.0 78.9 jit_solution(17756903012233851770)
XLA Ops:
  0.0 78.2 %shard_map.118 = bf16[192,512]{1,0:T(8,128)(2,1)S(1)} custom-call(bf16[192,384]{1,0:T(8,128)(2,1)} %q_in.1, bf16[4,48,512]{2,1,0:T(8,128)(2,1)} %bitcast.4, bf16[32,192]{1,0:T(8,128)(2,1)} %bitcast.5, bf16[512,256]{1,0:T(8,128)(2,1)} %wk_in.1, bf16[512,256]{1,0:T(8,128)(2,1)} %wv_in.1, bf16[256,2048]{1,0:T(8,128)(2,1)} %wo_ref.1, bf16[192,512]{1,0:T(8,128)(2,1)} %resid_in.1, ...), custom_call_target="tpu_custom_call" | custom-call | tf_op jit(solution)/shard_map/pallas_call | solution.py:1264
  78.2 0.7 copy.14

commit v6 on v5

--- a/solution.py
+++ b/solution.py
@@ -1198,8 +1198,8 @@
     each(pair_added, close, late)
     each(make_block, near, late)
     each(pair_first, rest + near, late)
+    each(pair_added, near + rest, early)
     each(add_far, close, early)
-    each(pair_added, near + rest, early)
     each(pair_added, rest + near, late)
     each(finish_far, close, late)
     each(finish_pair, close, early)

time: 79.1 us -> 79 us (level)
  no operation moved by 1% of the time
where the time goes in v6:
time: 79 us; the launch traced here: 78.6 us
  Pallas kernels  77.9 us (99%)
    pallas_call x1, Pallas kernels, paired_call(): pl.pallas_call(functools.partial(paired_kernel, n_sp, n_tp, pieces), out_...  77.9 us

profile of v6, /device:TPU:0, one launch (start us, length us, event | category | flops | bytes accessed | tf_op | source)
XLA Modules:
  0.0 78.6 jit_solution(2701311356232326191)
XLA Ops:
  0.0 77.9 %shard_map.118 = bf16[192,512]{1,0:T(8,128)(2,1)S(1)} custom-call(bf16[192,384]{1,0:T(8,128)(2,1)} %q_in.1, bf16[4,48,512]{2,1,0:T(8,128)(2,1)} %bitcast.4, bf16[32,192]{1,0:T(8,128)(2,1)} %bitcast.5, bf16[512,256]{1,0:T(8,128)(2,1)} %wk_in.1, bf16[512,256]{1,0:T(8,128)(2,1)} %wv_in.1, bf16[256,2048]{1,0:T(8,128)(2,1)} %wo_ref.1, bf16[192,512]{1,0:T(8,128)(2,1)} %resid_in.1, ...), custom_call_target="tpu_custom_call" | custom-call | tf_op jit(solution)/shard_map/pallas_call | solution.py:1264
  77.9 0.7 copy.14
